TPU v7x, 256 devices: a whole 4x4x8 slice. The times are simulated.
256 devices in a mesh: sp: 16 (over y, x), tp: 16 (over z, core).
Axes of the slice: x: 4, y: 4, z: 8, core: 2. Of those that a mesh axis runs over, the one named last changes fastest.
Arguments:
- residual_in: bfloat16 [4096, 4096], P(('sp', 'tp')), may hold values from -6 to 6
- queries: bfloat16 [4096, 2048], P('sp', 'tp'), may hold values from -6 to 6
- keys: bfloat16 [4096, 2048], P('sp', 'tp'), may hold values from -6 to 6
- values: bfloat16 [4096, 2048], P('sp', 'tp'), may hold values from -6 to 6
- break_offset: bfloat16 [4096, 32], P('sp', 'tp'), may hold values from -14 to 1
- doc_ids: int32 [4096], P('sp'), may hold values from 0 to 2, never falling along the last dimension, each value on 1 to 2560 neighbouring positions
- out_weight: bfloat16 [2048, 4096], P('tp'), may hold values from -0.125 to 0.125
- norm_gain: float32 [4096], replicated, may hold values from 0.1 to 1.9
- group_router: bfloat16 [4096, 2], replicated, may hold values from -0.1875 to 0.1875
- expert_router: bfloat16 [4096, 16], replicated, may hold values from -0.1875 to 0.1875
- expert_ids: int32 [4096, 2], P('sp'), may hold values from 0 to 15, as said below
- gate_weight: bfloat16 [16, 4096, 4096], P('sp', None, 'tp'), may hold values from -0.09375 to 0.09375
- up_weight: bfloat16 [16, 4096, 4096], P('sp', None, 'tp'), may hold values from -0.09375 to 0.09375
- down_weight: bfloat16 [16, 4096, 4096], P('sp', 'tp'), may hold values from -0.09375 to 0.09375
Outputs:
- layer_out: bfloat16 [4096, 4096], P(('sp', 'tp'))
Inputs may be any that keep to these rules, and one draw needn't show every extreme that they name: `doc_ids`: document numbers never fall along the positions; one document covers exactly 2560 positions. `expert_ids`: the two experts of a position differ and lie in one group of 8 consecutive numbers; in each aligned block of 16 positions every expert is named exactly 2 times.
All inputs are finite; a program needn't handle non-finite values.
Results may differ from a plain program's by a relative error of at most 0.013.
Values may be sent and summed in bfloat16 or wider, within the bound.
A program may use at most 64 MiB of HBM per device.

v0:
```python
import jax
import jax.numpy as jnp
from jax import lax
from jax.sharding import Mesh
from jax.sharding import PartitionSpec as P

HEAD_DIM = 64
GROUPS = 2
KEY_BLOCK = 256
TP = ("tp_0", "tp_1")
SP_TP = ("sp", "tp_0", "tp_1")


def in_one_piece(arrays, axis, dim, along):
    ends, at = ([], 0)
    for a in arrays[:-1]:
        at += a.shape[along]
        ends.append(at)
    both = jnp.concatenate(arrays, axis=along)
    return tuple(jnp.split(lax.all_gather(both, axis, axis=dim, tiled=True), ends, axis=along))


def cut_along(array, dim, count):
    before, after = (array.shape[:dim], array.shape[dim + 1 :])
    return jnp.moveaxis(array.reshape(*before, count, -1, *after), dim, 0)


def summed_on_arrival(array, axis, dim):
    blocks = cut_along(array, dim, lax.axis_size(axis))
    arrived = lax.all_to_all(blocks, axis, split_axis=0, concat_axis=0, tiled=True)
    return arrived.astype(jnp.float32).sum(axis=0)


def summed_rows(array, chips, core, dim):
    sizes = (lax.axis_size(chips), lax.axis_size(core))
    blocks = cut_along(array, dim, sizes[0] * sizes[1])
    inside = blocks.shape[1:]
    blocks = blocks.reshape(*sizes, *inside).swapaxes(0, 1).reshape(-1, *inside)
    blocks = lax.psum_scatter(blocks, core, scatter_dimension=0, tiled=True)
    return lax.psum_scatter(blocks, chips, scatter_dimension=0, tiled=True)[0]


def block_result(
    query_heads, key_block, value_block, offset_block, query_pos, query_doc, key_pos, key_doc
):
    scores = jnp.einsum(
        "qhd,khd->hqk", query_heads, key_block, preferred_element_type=jnp.float32
    ) * HEAD_DIM ** (-0.5)
    scores = scores + offset_block.astype(jnp.float32).T[:, None, :]
    live_mask = (
        (key_pos[None, :] < query_pos[:, None]) & (key_doc[None, :] == query_doc[:, None])
    )[None]
    stay_log = jnp.where(live_mask, jax.nn.log_sigmoid(-scores), jnp.float32(0.0))
    within = lax.cumsum(stay_log, axis=2, reverse=True) - stay_log
    weights = jnp.where(
        live_mask, jnp.exp(jax.nn.log_sigmoid(scores) + within), jnp.float32(0.0)
    ).astype(jnp.bfloat16)
    partial_out = jnp.einsum(
        "hqk,khd->hqd", weights, value_block, preferred_element_type=jnp.float32
    )
    return (partial_out, jnp.sum(stay_log, axis=2))


def normalize(rows, norm_gain):
    rows_f = rows.astype(jnp.float32)
    scaling = lax.rsqrt(jnp.mean(rows_f * rows_f, axis=1, keepdims=True) + 1e-06)
    return (rows_f * scaling * norm_gain[None, :]).astype(jnp.bfloat16)


def route_weights(normed, group_router, expert_router, chosen, group_size):
    group_logits = jnp.dot(normed, group_router, preferred_element_type=jnp.float32)
    expert_logits = jnp.dot(normed, expert_router, preferred_element_type=jnp.float32)
    chosen_group = chosen[:, 0] // group_size
    margin = group_logits[:, 0] - group_logits[:, 1]
    own_margin = jnp.where(chosen_group == 0, margin, -margin)
    experts_iota = jnp.arange(expert_logits.shape[1], dtype=jnp.int32)
    picked = jnp.sum(
        jnp.where(
            chosen[:, :, None] == experts_iota[None, None, :],
            expert_logits[:, None, :],
            jnp.float32(0.0),
        ),
        axis=2,
    )
    return jax.nn.sigmoid(own_margin)[:, None] * jax.nn.sigmoid(picked - picked[:, ::-1])


def slot_table(chosen, expert_count, slots):
    flat_ids = chosen.reshape(-1)
    onehot = (flat_ids[:, None] == jnp.arange(expert_count, dtype=jnp.int32)[None, :]).astype(
        jnp.int32
    )
    before = jnp.cumsum(onehot, axis=0) - onehot
    ranks = jnp.sum(before * onehot, axis=1)
    return (flat_ids * slots + ranks).reshape(chosen.shape)


def dispatch(normed, slot_ids, total_slots):
    flat_slots = slot_ids.reshape(-1)
    owners = jnp.arange(flat_slots.shape[0], dtype=jnp.int32) // 2
    slot_iota = jnp.arange(total_slots, dtype=jnp.int32)
    token_of_slot = jnp.sum(
        jnp.where(slot_iota[:, None] == flat_slots[None, :], owners[None, :], 0), axis=1
    )
    return jnp.take(normed, token_of_slot, axis=0)


def expert_rows(row_block, gate_part, up_part, down_part):
    gate_val = jnp.dot(row_block, gate_part, preferred_element_type=jnp.float32)
    up_val = jnp.dot(row_block, up_part, preferred_element_type=jnp.float32)
    hidden = (jax.nn.silu(gate_val) * up_val).astype(jnp.bfloat16)
    return jnp.dot(hidden, down_part, preferred_element_type=jnp.float32).astype(jnp.bfloat16)


def per_device(
    residual_in,
    queries,
    keys,
    values,
    break_offset,
    doc_ids,
    out_weight,
    norm_gain,
    group_router,
    expert_router,
    expert_ids,
    gate_weight,
    up_weight,
    down_weight,
):
    tok_dev = queries.shape[0]
    heads_dev = break_offset.shape[1]
    width = residual_in.shape[1]
    sp_count = lax.axis_size("sp")
    tp_count = lax.axis_size(TP)
    sp_rank = lax.axis_index("sp")
    tp_rank = lax.axis_index(TP)
    rows_dev = tok_dev // tp_count
    own_begin = tp_rank * rows_dev
    query_pos = sp_rank * tok_dev + jnp.arange(tok_dev, dtype=jnp.int32)
    query_heads = queries.reshape(tok_dev, heads_dev, HEAD_DIM)
    key_rows, value_rows, offset_rows, doc_rows = (
        *in_one_piece((keys, values, break_offset), "sp", 0, 1),
        lax.all_gather(doc_ids, "sp", axis=0, tiled=True),
    )
    length = key_rows.shape[0]
    block_count = length // KEY_BLOCK
    key_heads = key_rows.reshape(length, heads_dev, HEAD_DIM)
    value_heads = value_rows.reshape(length, heads_dev, HEAD_DIM)

    def advance(block_step, running_block):
        out_sum, stay_sum = running_block
        block_begin = (block_count - 1 - block_step) * KEY_BLOCK
        key_block = lax.dynamic_slice_in_dim(key_heads, block_begin, KEY_BLOCK, 0)
        value_block = lax.dynamic_slice_in_dim(value_heads, block_begin, KEY_BLOCK, 0)
        offset_block = lax.dynamic_slice_in_dim(offset_rows, block_begin, KEY_BLOCK, 0)
        key_doc = lax.dynamic_slice_in_dim(doc_rows, block_begin, KEY_BLOCK, 0)
        key_pos = block_begin + jnp.arange(KEY_BLOCK, dtype=jnp.int32)
        partial_out, totals = block_result(
            query_heads, key_block, value_block, offset_block, query_pos, doc_ids, key_pos, key_doc
        )
        return (out_sum + jnp.exp(stay_sum)[:, :, None] * partial_out, stay_sum + totals)

    initial = (
        jnp.zeros((heads_dev, tok_dev, HEAD_DIM), jnp.float32),
        jnp.zeros((heads_dev, tok_dev), jnp.float32),
    )
    out_sum, stay_sum = lax.fori_loop(0, block_count, advance, initial)
    slot = jnp.int32(0) // tok_dev
    slot_out = jnp.zeros((sp_count, heads_dev, tok_dev, HEAD_DIM), jnp.float32)
    slot_stay = jnp.zeros((sp_count, heads_dev, tok_dev), jnp.float32)
    slot_out = lax.dynamic_update_index_in_dim(slot_out, out_sum, slot, 0)
    slot_stay = lax.dynamic_update_index_in_dim(slot_stay, stay_sum, slot, 0)
    slot_out, slot_stay = (slot_out, slot_stay)
    later_stay = jnp.flip(jnp.cumsum(jnp.flip(slot_stay, 0), axis=0), 0) - slot_stay
    attended = jnp.sum(jnp.exp(later_stay)[..., None] * slot_out, axis=0)
    attended = (
        attended.transpose(1, 0, 2).reshape(tok_dev, heads_dev * HEAD_DIM).astype(jnp.bfloat16)
    )
    expert_count = sp_count * gate_weight.shape[0]
    group_size = expert_count // GROUPS
    summed = summed_on_arrival(
        jnp.dot(attended, out_weight, preferred_element_type=jnp.float32).astype(jnp.bfloat16),
        TP,
        0,
    )
    mixed_stream = (residual_in.astype(jnp.float32) + summed).astype(jnp.bfloat16)
    chosen = lax.dynamic_slice_in_dim(expert_ids, own_begin, rows_dev, 0)
    normed = normalize(mixed_stream, norm_gain)
    routes = route_weights(normed, group_router, expert_router, chosen, group_size)
    slots = 2 * rows_dev // expert_count
    slot_ids = slot_table(chosen, expert_count, slots)
    sent = dispatch(normed, slot_ids, expert_count * slots).reshape(expert_count, slots, width)
    fanned = lax.all_gather(
        lax.all_to_all(sent, "sp", split_axis=0, concat_axis=0, tiled=True), TP, axis=0, tiled=True
    )
    partial_out = expert_rows(
        fanned.reshape(-1, width), gate_weight[0], up_weight[0], down_weight[0]
    )
    unit_total = summed_rows(partial_out.reshape(fanned.shape), "tp_0", "tp_1", 0).astype(
        jnp.float32
    )
    returned = lax.all_to_all(
        unit_total.astype(jnp.bfloat16), "sp", split_axis=0, concat_axis=0, tiled=True
    )
    expert_out = jnp.take(returned.reshape(-1, width), slot_ids.reshape(-1), axis=0).reshape(
        rows_dev, 2, width
    )
    mixture = jnp.sum(routes[:, :, None] * expert_out.astype(jnp.float32), axis=1)
    return (mixed_stream.astype(jnp.float32) + mixture).astype(jnp.bfloat16)


def solution(mesh):
    finer = Mesh(mesh.devices.reshape(mesh.shape["sp"], 8, 2), ("sp", "tp_0", "tp_1"))
    in_specs = (
        P(SP_TP, None),
        P("sp", TP),
        P("sp", TP),
        P("sp", TP),
        P("sp", TP),
        P("sp"),
        P(TP, None),
        P(),
        P(),
        P(),
        P("sp", None),
        P("sp", None, TP),
        P("sp", None, TP),
        P("sp", TP, None),
    )
    out_specs = P(SP_TP, None)
    return jax.shard_map(
        per_device, mesh=finer, in_specs=in_specs, out_specs=out_specs, check_vma=False
    )
```

profile of v0, /device:TPU:1, one launch (start us, length us, event | category | flops | bytes accessed | tf_op | source)
XLA Modules:
  0.0 436.6 jit_solution(8774637428003538467)
XLA Ops:
  6.5 1.1 copy.67
  8.6 1.3 pad_maximum_fusion
  10.9 19.1 %all-gather = s32[16,1,256]{2,1,0:T(1,128)S(1)} all-gather(s32[1,1,256]{2,1,0:T(1,128)} %bitcast.87), channel_id=1, replica_groups=mesh['sp'=16,'tp_0'=8,'tp_1'=2] {'sp'}, dimensions={0}, use_global_device_ids=true | all-gather | bytes 17408 | tf_op jit(solution)/shard_map/all_gather | solution.py:144
  30.1 34.5 %all-gather.4.cloned.1.call-done = bf16[4096,258]{0,1:T(8,128)(2,1)} async-done(((bf16[256,258]{0,1:T(8,128)(2,1)}), bf16[4096,258]{0,1:T(8,128)(2,1)}) %all-gather.4.cloned.1.call-update) | async-done | bytes 2113552 | tf_op jit(solution)/shard_map/all_gather | solution.py:20
  64.6 3.1 fusion.48
  67.7 134.0 %while.16 = (s32[]{:T(128)}, f32[2,256,64]{1,2,0:T(8,128)S(1)}, f32[2,256]{1,0:T(2,128)S(1)}, s32[4096]{0:T(1024)S(1)}, s32[256]{0:T(256)S(1)}, /*index=5*/bf16[...) while((s32[]{:T(128)}, f32[2,256,64]{1,2,0:T(8,128)S(1)}, ...), condition=%wide.region_4.5_spmd.clone, body=%wide.region_0.4_spmd.clone.sunk | while | flops 54692872 | bytes 6479102 | solution.py:168
  67.9 1.4 fusion.76
  69.3 4.6 %fusion.77 = f32[2,256,2,128]{1,2,3,0:T(2,128)S(1)} fusion(f32[2,256,2,128]{1,3,2,0:T(8,128)S(1)} %bitcast.77), kind=kOutput, calls=%fused_computation.18.clone.1 | output fusion | flops 16646144 | bytes 1048576 | tf_op jit(solution)/shard_map/reduce-window.4
  75.0 1.0 fusion.80
  76.3 1.4 fusion.76
  77.7 4.6 %fusion.77 = f32[2,256,2,128]{1,2,3,0:T(2,128)S(1)} fusion(f32[2,256,2,128]{1,3,2,0:T(8,128)S(1)} %bitcast.77), kind=kOutput, calls=%fused_computation.18.clone.1 | output fusion | flops 16646144 | bytes 1048576 | tf_op jit(solution)/shard_map/reduce-window.4
  83.4 1.0 fusion.80
  84.6 1.4 fusion.76
  86.1 4.6 %fusion.77 = f32[2,256,2,128]{1,2,3,0:T(2,128)S(1)} fusion(f32[2,256,2,128]{1,3,2,0:T(8,128)S(1)} %bitcast.77), kind=kOutput, calls=%fused_computation.18.clone.1 | output fusion | flops 16646144 | bytes 1048576 | tf_op jit(solution)/shard_map/reduce-window.4
  91.7 1.0 fusion.80
  93.0 1.4 fusion.76
  94.5 4.6 %fusion.77 = f32[2,256,2,128]{1,2,3,0:T(2,128)S(1)} fusion(f32[2,256,2,128]{1,3,2,0:T(8,128)S(1)} %bitcast.77), kind=kOutput, calls=%fused_computation.18.clone.1 | output fusion | flops 16646144 | bytes 1048576 | tf_op jit(solution)/shard_map/reduce-window.4
  100.1 1.0 fusion.80
  101.4 1.4 fusion.76
  102.8 4.6 %fusion.77 = f32[2,256,2,128]{1,2,3,0:T(2,128)S(1)} fusion(f32[2,256,2,128]{1,3,2,0:T(8,128)S(1)} %bitcast.77), kind=kOutput, calls=%fused_computation.18.clone.1 | output fusion | flops 16646144 | bytes 1048576 | tf_op jit(solution)/shard_map/reduce-window.4
  109.8 1.4 fusion.76
  111.2 4.6 %fusion.77 = f32[2,256,2,128]{1,2,3,0:T(2,128)S(1)} fusion(f32[2,256,2,128]{1,3,2,0:T(8,128)S(1)} %bitcast.77), kind=kOutput, calls=%fused_computation.18.clone.1 | output fusion | flops 16646144 | bytes 1048576 | tf_op jit(solution)/shard_map/reduce-window.4
  116.9 1.0 fusion.80
  118.2 1.4 fusion.76
  119.6 4.6 %fusion.77 = f32[2,256,2,128]{1,2,3,0:T(2,128)S(1)} fusion(f32[2,256,2,128]{1,3,2,0:T(8,128)S(1)} %bitcast.77), kind=kOutput, calls=%fused_computation.18.clone.1 | output fusion | flops 16646144 | bytes 1048576 | tf_op jit(solution)/shard_map/reduce-window.4
  125.2 1.0 fusion.80
  126.5 1.4 fusion.76
  128.0 4.6 %fusion.77 = f32[2,256,2,128]{1,2,3,0:T(2,128)S(1)} fusion(f32[2,256,2,128]{1,3,2,0:T(8,128)S(1)} %bitcast.77), kind=kOutput, calls=%fused_computation.18.clone.1 | output fusion | flops 16646144 | bytes 1048576 | tf_op jit(solution)/shard_map/reduce-window.4
  133.6 1.0 fusion.80
  134.9 1.4 fusion.76
  136.4 4.6 %fusion.77 = f32[2,256,2,128]{1,2,3,0:T(2,128)S(1)} fusion(f32[2,256,2,128]{1,3,2,0:T(8,128)S(1)} %bitcast.77), kind=kOutput, calls=%fused_computation.18.clone.1 | output fusion | flops 16646144 | bytes 1048576 | tf_op jit(solution)/shard_map/reduce-window.4
  142.0 1.0 fusion.80
  143.3 1.4 fusion.76
  144.7 4.6 %fusion.77 = f32[2,256,2,128]{1,2,3,0:T(2,128)S(1)} fusion(f32[2,256,2,128]{1,3,2,0:T(8,128)S(1)} %bitcast.77), kind=kOutput, calls=%fused_computation.18.clone.1 | output fusion | flops 16646144 | bytes 1048576 | tf_op jit(solution)/shard_map/reduce-window.4
  150.4 1.0 fusion.80
  151.7 1.4 fusion.76
  153.1 4.6 %fusion.77 = f32[2,256,2,128]{1,2,3,0:T(2,128)S(1)} fusion(f32[2,256,2,128]{1,3,2,0:T(8,128)S(1)} %bitcast.77), kind=kOutput, calls=%fused_computation.18.clone.1 | output fusion | flops 16646144 | bytes 1048576 | tf_op jit(solution)/shard_map/reduce-window.4
  158.8 1.0 fusion.80
  160.1 1.4 fusion.76
  161.5 4.6 %fusion.77 = f32[2,256,2,128]{1,2,3,0:T(2,128)S(1)} fusion(f32[2,256,2,128]{1,3,2,0:T(8,128)S(1)} %bitcast.77), kind=kOutput, calls=%fused_computation.18.clone.1 | output fusion | flops 16646144 | bytes 1048576 | tf_op jit(solution)/shard_map/reduce-window.4
  168.4 1.4 fusion.76
  169.9 4.6 %fusion.77 = f32[2,256,2,128]{1,2,3,0:T(2,128)S(1)} fusion(f32[2,256,2,128]{1,3,2,0:T(8,128)S(1)} %bitcast.77), kind=kOutput, calls=%fused_computation.18.clone.1 | output fusion | flops 16646144 | bytes 1048576 | tf_op jit(solution)/shard_map/reduce-window.4
  176.8 1.4 fusion.76
  178.2 4.6 %fusion.77 = f32[2,256,2,128]{1,2,3,0:T(2,128)S(1)} fusion(f32[2,256,2,128]{1,3,2,0:T(8,128)S(1)} %bitcast.77), kind=kOutput, calls=%fused_computation.18.clone.1 | output fusion | flops 16646144 | bytes 1048576 | tf_op jit(solution)/shard_map/reduce-window.4
  185.2 1.4 fusion.76
  186.6 4.6 %fusion.77 = f32[2,256,2,128]{1,2,3,0:T(2,128)S(1)} fusion(f32[2,256,2,128]{1,3,2,0:T(8,128)S(1)} %bitcast.77), kind=kOutput, calls=%fused_computation.18.clone.1 | output fusion | flops 16646144 | bytes 1048576 | tf_op jit(solution)/shard_map/reduce-window.4
  193.6 1.4 fusion.76
  195.0 4.6 %fusion.77 = f32[2,256,2,128]{1,2,3,0:T(2,128)S(1)} fusion(f32[2,256,2,128]{1,3,2,0:T(8,128)S(1)} %bitcast.77), kind=kOutput, calls=%fused_computation.18.clone.1 | output fusion | flops 16646144 | bytes 1048576 | tf_op jit(solution)/shard_map/reduce-window.4
  202.0 3.2 convolution_convert_fusion.1
  205.2 9.4 %all-to-all-start = ((bf16[16,16,4096]{2,1,0:T(8,128)(2,1)}), bf16[16,16,4096]{2,1,0:T(8,128)(2,1)}, u32[]{:S(2)}, u32[]{:S(2)}) async-start(bf16[16,16,4096]{2,1,0:T(8,128)(2,1)} %bitcast.78), calls=%async_computation | async-start | bytes 4194304 | tf_op jit(solution)/shard_map/all_to_all | solution.py:30
  215.7 48.1 %all-to-all-done = bf16[16,16,4096]{2,1,0:T(8,128)(2,1)} async-done(((bf16[16,16,4096]{2,1,0:T(8,128)(2,1)}), bf16[16,16,4096]{2,1,0:T(8,128)(2,1)}, u32[]{:S(2)}, u32[]{:S(2)}) %all-to-all-start) | async-done | bytes 2097184 | tf_op jit(solution)/shard_map/all_to_all | solution.py:30
  263.8 1.9 convert_reduce_fusion
  267.2 12.8 %all_to_all.15 = bf16[16,2,4096]{2,1,0:T(2,128)(2,1)} all-to-all(bf16[16,2,4096]{2,1,0:T(2,128)(2,1)S(1)} %broadcast_select_fusion.1), channel_id=1, replica_groups=mesh['sp'=16,'tp_0'=8,'tp_1'=2] {'sp'}, dimensions={0} | all-to-all | bytes 524288 | tf_op jit(solution)/shard_map/all_to_all | solution.py:195
  280.3 38.0 %all-gather.6.cloned.1.call-done = bf16[256,2,4096]{2,1,0:T(2,128)(2,1)} async-done(((bf16[16,2,4096]{2,1,0:T(2,128)(2,1)}), bf16[256,2,4096]{2,1,0:T(2,128)(2,1)}) %all-gather.6.cloned.1.call-update) | async-done | bytes 4194320 | tf_op jit(solution)/shard_map/all_gather | solution.py:194
  318.2 7.2 %reshape.213 = bf16[512,4096]{1,0:T(8,128)(2,1)} reshape(bf16[256,2,4096]{2,1,0:T(2,128)(2,1)} %all-gather.6.cloned.1.call-done) | data formatting | bytes 8388608 | tf_op jit(solution)/shard_map/reshape | solution.py:198
  325.4 4.1 fusion.24
  329.5 9.3 %convolution_convert_fusion = bf16[512,4096]{1,0:T(8,128)(2,1)} fusion(bf16[1,256,4096]{2,1,0:T(8,128)(2,1)S(1)} %copy-done, bf16[512,4096]{1,0:T(8,128)(2,1)} %reshape.213, bf16[1,4096,256]{2,1,0:T(8,128)(2,1)} %param.28, f32[512,256]{1,0:T(8,128)S(1)} %fusion.24), kind=kOutput, calls=%fused_computation.34 | convolution fusion | flops 2150367232 | bytes 13107200 | tf_op jit(solution)/shard_map/dot_general | solution.py:112
  338.8 7.6 %reshape_reshape_reshape.3 = bf16[8,2,16,2,4096]{4,3,2,1,0:T(2,128)(2,1)} reshape(bf16[512,4096]{1,0:T(8,128)(2,1)} %convolution_convert_fusion) | data formatting | bytes 8388608 | tf_op jit(solution)/shard_map/reshape;reshape;reshape | solution.py:38
  346.4 7.0 %copy.78 = bf16[8,2,16,2,4096]{4,2,3,0,1:T(8,128)(2,1)} copy(bf16[8,2,16,2,4096]{4,3,2,1,0:T(2,128)(2,1)} %reshape_reshape_reshape.3) | data formatting | bytes 8388608 | tf_op jit(solution)/shard_map/reshape;reshape;reshape | solution.py:38
  353.6 16.4 %reduce-scatter.3.cloned.1.call-done = bf16[8,16,2,4096]{3,1,2,0:T(8,128)(2,1)} async-done(((bf16[16,16,2,4096]{3,1,2,0:T(8,128)(2,1)}), bf16[8,16,2,4096]{3,1,2,0:T(8,128)(2,1)}) %reduce-scatter.3.cloned.1.call-update) | async-done | bytes 2097168 | tf_op jit(solution)/shard_map/reduce_scatter | solution.py:39
  370.8 40.7 %reduce-scatter.5.cloned.1.call-done = bf16[1,16,2,4096]{3,1,2,0:T(8,128)(2,1)} async-done(((bf16[8,16,2,4096]{3,1,2,0:T(8,128)(2,1)}), bf16[1,16,2,4096]{3,1,2,0:T(8,128)(2,1)}) %reduce-scatter.5.cloned.1.call-update) | async-done | bytes 262160 | tf_op jit(solution)/shard_map/reduce_scatter | solution.py:40
  411.5 1.9 copy.79
  413.4 6.5 %all-to-all-start.2 = ((bf16[16,2,4096]{2,1,0:T(2,128)(2,1)}), bf16[16,2,4096]{2,1,0:T(2,128)(2,1)S(1)}, u32[]{:S(2)}, u32[]{:S(2)}) async-start(bf16[16,2,4096]{2,1,0:T(2,128)(2,1)} %copy.79), calls=%async_computation.4 | async-start | bytes 524288 | tf_op jit(solution)/shard_map/all_to_all | solution.py:203
  420.3 7.3 %all-to-all-done.2 = bf16[16,2,4096]{2,1,0:T(2,128)(2,1)S(1)} async-done(((bf16[16,2,4096]{2,1,0:T(2,128)(2,1)}), bf16[16,2,4096]{2,1,0:T(2,128)(2,1)S(1)}, u32[]{:S(2)}, u32[]{:S(2)}) %all-to-all-start.2) | async-done | bytes 262176 | tf_op jit(solution)/shard_map/all_to_all | solution.py:203
  (255 shorter events, 34.6 us)
Async XLA Ops:
  6.5 323.0 %copy-start = (bf16[1,256,4096]{2,1,0:T(8,128)(2,1)S(1)}, bf16[1,256,4096]{2,1,0:T(8,128)(2,1)}, u32[]{:S(2)}) copy-start(bf16[1,256,4096]{2,1,0:T(8,128)(2,1)} %param.29) | copy-start | bytes 6291460
  6.5 58.0 %all-gather.4.cloned.1.call-start = ((), (), s32[]{:S(2)}) async-start(), calls=%async_computation.5 | async-start | bytes 2297856 | tf_op jit(solution)/shard_map/all_gather | solution.py:20
  64.6 3.1 slice-start
  64.6 3.1 copy-start.3
  205.2 9.5 %copy-start.5 = (s32[256,2]{0,1:T(2,128)S(1)}, s32[256,2]{0,1:T(2,128)}, u32[]{:S(2)}) copy-start(s32[256,2]{0,1:T(2,128)} %param.26) | copy-start | bytes 6148
  205.2 58.6 %all-to-all-start = ((bf16[16,16,4096]{2,1,0:T(8,128)(2,1)}), bf16[16,16,4096]{2,1,0:T(8,128)(2,1)}, u32[]{:S(2)}, u32[]{:S(2)}) async-start(bf16[16,16,4096]{2,1,0:T(8,128)(2,1)} %bitcast.78), calls=%async_computation | async-start | bytes 4194304 | tf_op jit(solution)/shard_map/all_to_all | solution.py:30
  214.6 51.1 %copy-start.1 = (bf16[16,4096]{1,0:T(8,128)(2,1)S(1)}, bf16[16,4096]{1,0:T(8,128)(2,1)}, u32[]{:S(2)}) copy-start(bf16[16,4096]{1,0:T(8,128)(2,1)} %param.16) | copy-start | bytes 393220
  214.6 51.3 %copy-start.4 = (f32[4096]{0:T(1024)S(1)}, f32[4096]{0:T(1024)}, u32[]{:S(2)}) copy-start(f32[4096]{0:T(1024)} %param.23) | copy-start | bytes 49156
  214.7 103.6 %all-gather.6.cloned.1.call-start = ((), (), s32[]{:S(2)}) async-start(), calls=%async_computation.6 | async-start | bytes 4456448 | tf_op jit(solution)/shard_map/all_gather | solution.py:194
  280.0 89.9 %reduce-scatter.3.cloned.1.call-start = ((), (), s32[]{:S(2)}) async-start(), calls=%async_computation.7 | async-start | bytes 6291456 | tf_op jit(solution)/shard_map/reduce_scatter | solution.py:39
  353.5 17.0 %copy-start.6 = (bf16[4096,2]{0,1:T(2,128)(2,1)S(1)}, bf16[4096,2]{0,1:T(2,128)(2,1)}, u32[]{:S(2)}) copy-start(bf16[4096,2]{0,1:T(2,128)(2,1)} %param.24) | copy-start | bytes 49156
  353.5 17.1 %copy-start.2 = (bf16[4096,16]{0,1:T(8,128)(2,1)S(1)}, bf16[4096,16]{0,1:T(8,128)(2,1)}, u32[]{:S(2)}) copy-start(bf16[4096,16]{0,1:T(8,128)(2,1)} %param.25) | copy-start | bytes 393220
  353.5 58.0 %reduce-scatter.5.cloned.1.call-start = ((), (), s32[]{:S(2)}) async-start(), calls=%async_computation.8 | async-start | bytes 2359296 | tf_op jit(solution)/shard_map/reduce_scatter | solution.py:40
  413.4 14.1 %all-to-all-start.2 = ((bf16[16,2,4096]{2,1,0:T(2,128)(2,1)}), bf16[16,2,4096]{2,1,0:T(2,128)(2,1)S(1)}, u32[]{:S(2)}, u32[]{:S(2)}) async-start(bf16[16,2,4096]{2,1,0:T(2,128)(2,1)} %copy.79), calls=%async_computation.4 | async-start | bytes 524288 | tf_op jit(solution)/shard_map/all_to_all | solution.py:203
Sparse Core Ops, SparseCore 0:
  10.1 54.4 all-gather.3
  280.1 38.0 all-gather.5
  353.6 16.2 reduce-scatter.2
  372.3 39.1 reduce-scatter.4
where the time goes:
time: 443 us; the launch traced here: 437 us
  waiting for transfers between devices  185 us (42%)
  other arithmetic  97.7 us (22%)
  matrix products  56.4 us (13%)
  local copies, waits for them, and re-layouts  34.8 us (8%)
  blocking collectives  31.9 us (7%)
  starting transfers between devices  16.3 us (4%)
  between operations  13.4 us (3%)
    another operation x32, other arithmetic  74.1 us
    all_to_all x1, waiting for transfers between devices, summed_on_arrival(): lax.all_to_all(blocks, axis, split_axis=0, concat_axis=0, tiled=True)  48.1 us
    reduce_scatter x1, waiting for transfers between devices, summed_rows(): return lax.psum_scatter(blocks, chips, scatter_dimension=0, tiled=True)[0]  40.7 us
    all_gather x1, waiting for transfers between devices, per_device(): lax.all_gather(lax.all_to_all(sent, 'sp', split_axis=0, concat_axis=0, ti...  38 us
    all_gather x1, waiting for transfers between devices, in_one_piece(): lax.all_gather(both, axis, axis=dim, tiled=True)  34.5 us
    dot_general x16, matrix products, block_result(): jnp.einsum('qhd,khd->hqk', query_heads, key_block, preferred_element_type...  22.9 us
    all_gather x1, blocking collectives, per_device(): lax.all_gather(doc_ids, 'sp', axis=0, tiled=True)  19.1 us
    dot_general x16, matrix products, block_result(): jnp.einsum('hqk,khd->hqd', weights, value_block, preferred_element_type=j...  16.5 us
  transfers between devices with their start and end apart: 6, of which 6 were waited for; matrix products, arithmetic and copies ran while one was open for 1% of the time, Pallas kernels for 0%

commit v1 on v0

v1 whole, which is shorter than its diff:
```python
import functools

import jax
import jax.numpy as jnp
from jax import lax
from jax.experimental import pallas as pl
from jax.experimental.pallas import tpu as pltpu
from jax.sharding import Mesh
from jax.sharding import PartitionSpec as P

HEAD_DIM = 64
GROUPS = 2
DOC_MOST = 2560
KB = 256
MESH = pl.DeviceIdType.MESH
AXES = ("y", "x", "z", "c")
SP = ("y", "x")
TP = ("z", "c")
VM = pl.BlockSpec(memory_space=pltpu.VMEM)
ANY = pl.BlockSpec(memory_space=pl.ANY)
BF = jnp.bfloat16
F32 = jnp.float32
LIMIT = 60 * 1024 * 1024


def dot(a, b):
    return jnp.dot(a, b, preferred_element_type=F32)


def place():
    return tuple(lax.axis_index(a) for a in AXES)


def remote(src, dst, ss, rs, to):
    return pltpu.make_async_remote_copy(
        src_ref=src, dst_ref=dst, send_sem=ss, recv_sem=rs, device_id=to, device_id_type=MESH
    )


def greet(peers):
    bar = pltpu.get_barrier_semaphore()
    for p in peers:
        pl.semaphore_signal(bar, inc=1, device_id=p, device_id_type=MESH)
    pl.semaphore_wait(bar, len(peers))


def gather_kernel(band, ny, nx, k, v, a, w, ko, vo, ao, wo, ks, kr, vs, vr, as_, ar, ws, wr):
    y, x, z, c = place()
    me = y * nx + x
    xs = [lax.rem(x + d, nx) for d in range(1, nx)]
    ys = [lax.rem(y + d, ny) for d in range(1, ny)]
    xb = [lax.rem(x + nx - d, nx) for d in range(1, nx)]
    yb = [lax.rem(y + ny - d, ny) for d in range(1, ny)]
    half = wo.shape[1]
    greet(
        [(y, q, z, c) for q in xs] + [(q, x, z, c) for q in ys] + [(y, x, z, 1 - c)]
    )

    def used(b, j):
        return (j > b) & (j - b <= band)

    def k_first(xs_, xd):
        return (xd > xs_) | (y < ny - 1)

    def v_first(yd, ys_, xs_):
        return (yd > ys_) & (nx * (yd - ys_) - xs_ <= band)

    wcopy = remote(w.at[:, pl.ds((1 - c) * half, half)], wo, ws, wr, (y, x, z, 1 - c))

    def kcopy(b, src, asrc, n, to):
        return (
            remote(src, ko.at[b], ks.at[n], kr.at[b], to),
            remote(asrc, ao.at[b], as_.at[n], ar.at[b], to),
        )

    def vcopy(b, src, n, to):
        return (remote(src, vo.at[b], vs.at[n], vr.at[b], to),)

    plan = []
    wants = []

    def send(cond, copies):
        plan.append((cond, copies))

        @pl.when(cond)
        def _():
            for q in copies:
                q.start()

    def arrive(cond, copies):
        @pl.when(cond)
        def _():
            for q in copies:
                q.wait_recv()

    n = 0
    for q in xs:
        send(k_first(x, q), kcopy(me, k, a, n, (y, q, z, c)))
        n += 1
    m = 0
    for q in ys:
        send(v_first(q, y, x), vcopy(me, v, m, (q, x, z, c)))
        m += 1
    for q in ys:
        send(used(me, q * nx + x), kcopy(me, k, a, n, (q, x, z, c)))
        n += 1
    for q in xs:
        send(used(me, y * nx + q), vcopy(me, v, m, (y, q, z, c)))
        m += 1
    wcopy.start()
    ko[me] = k[...]
    vo[me] = v[...]
    ao[me] = a[...]
    for i in range(max(nx, ny) - 1):
        if i < nx - 1:
            b = y * nx + xb[i]
            got = k_first(xb[i], x)
            arrive(got, kcopy(b, k, a, 0, (y, x, z, c)))
            for q in ys:
                send(got & used(b, q * nx + x), kcopy(b, ko.at[b], ao.at[b], n, (q, x, z, c)))
                n += 1
        if i < ny - 1:
            b = yb[i] * nx + x
            got = v_first(y, yb[i], x)
            arrive(got, vcopy(b, v, 0, (y, x, z, c)))
            for q in xs:
                send(got & used(b, y * nx + q), vcopy(b, vo.at[b], m, (y, q, z, c)))
                m += 1
    for qy in yb:
        for qx in [x] + xb:
            b = qy * nx + qx
            arrive(used(b, me), kcopy(b, k, a, 0, (y, x, z, c)))
    for qx in xb:
        for qy in [y] + yb:
            b = qy * nx + qx
            arrive(used(b, me), vcopy(b, v, 0, (y, x, z, c)))
    for cond, copies in plan:

        @pl.when(cond)
        def _(copies=copies):
            for q in copies:
                q.wait_send()

    wcopy.wait()


def gather_keys(k, v, a, w, ny, nx, cid):
    n = ny * nx
    sends = (nx - 1) + (ny - 1) + (nx - 1) * (ny - 1)
    half = w.shape[1] // 2
    dma = pltpu.SemaphoreType.DMA
    return pl.pallas_call(
        functools.partial(gather_kernel, DOC_MOST // KB, ny, nx),
        out_shape=(
            jax.ShapeDtypeStruct((n,) + k.shape, BF),
            jax.ShapeDtypeStruct((n,) + v.shape, BF),
            jax.ShapeDtypeStruct((n,) + a.shape, BF),
            jax.ShapeDtypeStruct((w.shape[0], half), BF),
        ),
        in_specs=[VM, VM, VM, VM],
        out_specs=(VM, VM, VM, VM),
        scratch_shapes=[
            dma((sends,)), dma((n,)), dma((sends,)), dma((n,)), dma((sends,)), dma((n,)), dma, dma,
        ],
        compiler_params=pltpu.CompilerParams(
            collective_id=cid, has_side_effects=True, vmem_limit_bytes=LIMIT
        ),
        name="gather_keys",
    )(k, v, a, w)


def attend_kernel(band, nx, q, k, v, a, qdoc, o):
    y, x, z, c = place()
    me = y * nx + x
    rows = q.shape[0]
    heads = q.shape[1] // HEAD_DIM
    tri_r = lax.broadcasted_iota(jnp.int32, (KB, KB), 0)
    tri_c = lax.broadcasted_iota(jnp.int32, (KB, KB), 1)
    later = (tri_r > tri_c).astype(BF)
    qh = [q[:, h * HEAD_DIM : (h + 1) * HEAD_DIM] * BF(HEAD_DIM**-0.5) for h in range(heads)]
    qd = qdoc[...]

    def step(t, carry):
        b = me - t
        kb = k[b]
        vb = v[b]
        ab = a[b].astype(F32)
        live = ab[heads : heads + 1, :] == qd
        live = live & ((t > 0) | (tri_c < tri_r))
        new = []
        for h in range(heads):
            out, stay_sum = carry[h]
            kh = kb[:, h * HEAD_DIM : (h + 1) * HEAD_DIM]
            vh = vb[:, h * HEAD_DIM : (h + 1) * HEAD_DIM]
            s = lax.dot_general(
                qh[h], kh, (((1,), (1,)), ((), ())), preferred_element_type=F32
            )
            s = s + ab[h : h + 1, :]
            soft = jnp.log1p(jnp.exp(-jnp.abs(s)))
            stay = jnp.where(live, -(jnp.maximum(s, 0.0) + soft), 0.0)
            hi = stay.astype(BF)
            lo = (stay - hi.astype(F32)).astype(BF)
            within = dot(hi, later) + dot(lo, later)
            wt = jnp.where(live, jnp.exp(jnp.minimum(s, 0.0) - soft + within), 0.0).astype(BF)
            out = out + jnp.exp(stay_sum) * dot(wt, vh)
            stay_sum = stay_sum + jnp.sum(stay, axis=1, keepdims=True)
            new.append((out, stay_sum))
        return tuple(new)

    zero = tuple(
        (jnp.zeros((rows, HEAD_DIM), F32), jnp.zeros((rows, 1), F32)) for _ in range(heads)
    )
    done = lax.fori_loop(0, jnp.minimum(me, band) + 1, step, zero)
    for h in range(heads):
        o[:, h * HEAD_DIM : (h + 1) * HEAD_DIM] = done[h][0].astype(BF)


def attend(q, k, v, a, qdoc, nx):
    return pl.pallas_call(
        functools.partial(attend_kernel, DOC_MOST // KB, nx),
        out_shape=jax.ShapeDtypeStruct(q.shape, BF),
        in_specs=[VM] * 5,
        out_specs=VM,
        compiler_params=pltpu.CompilerParams(vmem_limit_bytes=LIMIT),
        name="attend",
    )(q, k, v, a, qdoc)


def ring_ids(z, nz):
    return lax.rem(z + 1, nz), lax.rem(z + nz - 1, nz)


def project_kernel(nz, nsub, att, w, wsib, res, out, pair, part, sbuf, rbuf, xbuf, ybuf,
                   ds, dr, ss, rs, es, er):
    y, x, z, c = place()
    right, left = ring_ids(z, nz)
    sib = (y, x, z, 1 - c)
    half = w.shape[1] // 2
    kd = att.shape[1]
    greet([(y, x, right, c), (y, x, left, c), sib])
    first = remote(att, pair, ds, dr, sib)
    first.start()
    rows = att.shape[0]
    chunk = rows // nz
    hr = chunk // 2
    part[...] = dot(att[...], w[:, pl.ds(pl.multiple_of(c * half, half), half)])
    first.wait()
    part[...] += dot(pair[...], wsib[...])
    width = half // nsub

    def ring(d, s, j):
        to = right if d == 0 else left
        return remote(
            sbuf.at[d, s, :, pl.ds(j * width, width)],
            rbuf.at[d, s, :, pl.ds(j * width, width)],
            ss.at[d, s, j],
            rs.at[d, s, j],
            (y, x, to, c),
        )

    def own(d, s, j):
        zz = lax.rem(z + nz - 1 - s, nz) if d == 0 else lax.rem(z + 1 + s, nz)
        begin = pl.multiple_of(zz * chunk + d * hr, hr)
        return part[pl.ds(begin, hr), j * width : (j + 1) * width]

    for s in range(nz - 1):
        for j in range(nsub):
            for d in range(2):
                cols = slice(j * width, (j + 1) * width)
                val = own(d, s, j)
                if s > 0:
                    ring(d, s - 1, j).wait_recv()
                    val = val + rbuf[d, s - 1, :, cols].astype(F32)
                sbuf[d, s, :, cols] = val.astype(BF)
                ring(d, s, j).start()
    swap = remote(xbuf, ybuf, es, er, sib)
    mine = []
    for d in range(2):
        tot = []
        for j in range(nsub):
            cols = slice(j * width, (j + 1) * width)
            ring(d, nz - 2, j).wait_recv()
            tot.append(own(d, nz - 1, j) + rbuf[d, nz - 2, :, cols].astype(F32))
        mine.append(jnp.concatenate(tot, axis=1))
    keep = jnp.where(c == 0, mine[0], mine[1])
    xbuf[...] = jnp.where(c == 0, mine[1], mine[0])
    swap.start()
    swap.wait()
    got = ybuf[...]
    low = jnp.where(c == 0, keep, got)
    high = jnp.where(c == 0, got, keep)
    out[:, :half] = (res[:, :half].astype(F32) + low).astype(BF)
    out[:, half:] = (res[:, half:].astype(F32) + high).astype(BF)
    for s in range(nz - 1):
        for j in range(nsub):
            for d in range(2):
                ring(d, s, j).wait_send()


def project(att, w, wsib, res, nz, cid):
    half = w.shape[1] // 2
    hr = att.shape[0] // nz // 2
    nsub = 2
    dma = pltpu.SemaphoreType.DMA
    return pl.pallas_call(
        functools.partial(project_kernel, nz, nsub),
        out_shape=jax.ShapeDtypeStruct(res.shape, BF),
        in_specs=[VM] * 4,
        out_specs=VM,
        scratch_shapes=[
            pltpu.VMEM(att.shape, BF),
            pltpu.VMEM((att.shape[0], half), F32),
            pltpu.VMEM((2, nz - 1, hr, half), BF),
            pltpu.VMEM((2, nz - 1, hr, half), BF),
            pltpu.VMEM((hr, half), F32),
            pltpu.VMEM((hr, half), F32),
            dma, dma,
            dma((2, nz - 1, nsub)), dma((2, nz - 1, nsub)),
            dma, dma,
        ],
        compiler_params=pltpu.CompilerParams(
            collective_id=cid, has_side_effects=True, vmem_limit_bytes=LIMIT
        ),
        name="project",
    )(att, w, wsib, res)


def expert_kernel(ny, nx, nz, nsub, sent, gate, up, down, out,
                  gw, uw, dw, dsib, inb, rows, hid, sbuf, rbuf, fin, lsem,
                  ws, wr, is_, ir, gs, gr, cs, cr, hs, hr_, ss, rs, fs, fr):
    y, x, z, c = place()
    me = y * nx + x
    n = ny * nx
    right, left = ring_ids(z, nz)
    sib = (y, x, z, 1 - c)
    units = dw.shape[0]
    half = dw.shape[1]
    width_all = 2 * half
    per = 2 * n
    loads = [
        pltpu.make_async_copy(gate, gw, lsem.at[0]),
        pltpu.make_async_copy(up, uw, lsem.at[1]),
        pltpu.make_async_copy(
            down.at[:, pl.ds(pl.multiple_of(c * half, half), half)], dw, lsem.at[2]
        ),
    ]
    for q in loads:
        q.start()
    others = []
    for d in range(1, n):
        t = lax.rem(me + d, n)
        others.append((lax.div(t, nx), lax.rem(t, nx), t))
    greet(
        [(ty, tx, z, c) for ty, tx, t in others]
        + [(ty, tx, z, 1 - c) for ty, tx, t in others]
        + [(y, x, right, c), (y, x, left, c), sib]
    )
    wcopy = remote(
        down.at[:, pl.ds(pl.multiple_of((1 - c) * half, half), half)], dsib, ws, wr, sib
    )
    for d, (ty, tx, t) in enumerate(others):
        remote(sent.at[t], inb.at[me], is_.at[d], ir.at[me], (ty, tx, z, c)).start()
    wcopy.start()
    inb[me] = sent[me]
    for ty, tx, t in others:
        remote(sent.at[t], inb.at[t], is_.at[0], ir.at[t], (y, x, z, c)).wait_recv()
    mine = z * 2 + c
    for e in range(n):
        rows[mine, 2 * e : 2 * e + 2, :] = inb[e]

    hb = per // 2

    def piece(b, p):
        return rows.at[b, pl.ds(p * hb, hb), :]

    def hop(d, h, p):
        zz = lax.rem(z + nz - (h - 1), nz) if d == 0 else lax.rem(z + h - 1, nz)
        to = right if d == 0 else left
        b = zz * 2 + c
        return remote(piece(b, p), piece(b, p), gs.at[d, h, p], gr.at[d, h, p], (y, x, to, c))

    def got(d, h, p):
        zz = lax.rem(z + nz - h, nz) if d == 0 else lax.rem(z + h, nz)
        b = zz * 2 + c
        to = right if d == 0 else left
        return b, remote(piece(b, p), piece(b, p), gs.at[d, h, p], gr.at[d, h, p], (y, x, to, c))

    def cross(b, d, h, p):
        return remote(piece(b, p), piece(b, p), cs.at[d, h, p], cr.at[d, h, p], sib)

    def cross_from(d, h, p):
        zz = lax.rem(z + nz - h, nz) if d == 0 else lax.rem(z + h, nz)
        b = zz * 2 + (1 - c)
        return remote(piece(b, p), piece(b, p), cs.at[d, h, p], cr.at[d, h, p], sib)

    far = nz // 2
    sends = []

    def pieces(d, h):
        return (0, 1) if h < far else ((0,) if d == 0 else (1,))

    for p in (0, 1):
        for d in (0, 1):
            q = hop(d, 1, p)
            q.start()
            sends.append(q)
    for p in (0, 1):
        q = cross(mine, 0, 0, p)
        q.start()
        sends.append(q)

    def expert(blocks):
        xin = jnp.concatenate([rows[b] for b in blocks], axis=0)
        g = dot(xin, gw[...])
        u = dot(xin, uw[...])
        hval = (g * jax.nn.sigmoid(g) * u).astype(BF)
        for i, b in enumerate(blocks):
            hid[0, b] = hval[i * per : (i + 1) * per]

    def hswap(b, k):
        return remote(hid.at[0, b], hid.at[1, b], hs.at[k], hr_.at[k], sib)

    def blocks_of(h):
        if h == 0:
            return [(z * 2 + 0, 0), (z * 2 + 1, 1)]
        lo = lax.rem(z + nz - h, nz)
        hi = lax.rem(z + h, nz)
        if h == far:
            return [(lo * 2 + k, 4 * h - 2 + k) for k in (0, 1)]
        return [(lo * 2 + k, 4 * h - 2 + k) for k in (0, 1)] + [
            (hi * 2 + k, 4 * h + k) for k in (0, 1)
        ]

    def run(h):
        bl = blocks_of(h)
        expert([b for b, k in bl])
        for b, k in bl:
            q = hswap(b, k)
            q.start()
            sends.append(q)
        for b, k in bl:
            hswap(b, k).wait_recv()

    width = half // nsub

    def ring(d, s, j):
        to = right if d == 0 else left
        return remote(
            sbuf.at[d, s, :, pl.ds(j * width, width)],
            rbuf.at[d, s, :, pl.ds(j * width, width)],
            ss.at[d, s, j],
            rs.at[d, s, j],
            (y, x, to, c),
        )

    def own(d, s):
        zz = lax.rem(z + nz - 1 - s, nz) if d == 0 else lax.rem(z + 1 + s, nz)
        b = zz * 2 + d
        return dot(hid[0, b], dw[...]) + dot(hid[1, b], dsib[...])

    def own_pair(d, s):
        zz = lax.rem(z + nz - 1 - s, nz) if d == 0 else lax.rem(z + 1 + s, nz)
        b = zz * 2 + d
        return hid[0, b], hid[1, b]

    def partial(d, s):
        h0, h1 = own_pair(d, s)
        first = jnp.where(c == 0, 1, 0)
        del first
        return dot(h0, dw[...]) + dot(h1, dsib[...])

    def reduce_step(s):
        for d in range(2):
            val = partial(d, s)
            for j in range(nsub):
                cols = slice(j * width, (j + 1) * width)
                v = val[:, cols]
                if s > 0:
                    ring(d, s - 1, j).wait_recv()
                    v = v + rbuf[d, s - 1, :, cols].astype(F32)
                sbuf[d, s, :, cols] = v.astype(BF)
                q = ring(d, s, j)
                q.start()
                sends.append(q)

    for q in loads[:2]:
        q.wait()
    for p in (0, 1):
        cross_from(0, 0, p).wait_recv()
    run(0)
    loads[2].wait()
    wcopy.wait_recv()
    for h in range(1, far + 1):
        for p in (0, 1):
            for d in (0, 1):
                if p not in pieces(d, h):
                    continue
                b, q = got(d, h, p)
                q.wait_recv()
                if h + 1 <= far and p in pieces(d, h + 1):
                    f = hop(d, h + 1, p)
                    f.start()
                    sends.append(f)
                f = cross(b, d, h, p)
                f.start()
                sends.append(f)
        for p in (0, 1):
            for d in (0, 1):
                if p in pieces(d, h):
                    cross_from(d, h, p).wait_recv()
        run(h)
        reduce_step(h - 1)
    for s in range(far, nz - 1):
        reduce_step(s)
    for d in range(2):
        val = partial(d, nz - 1)
        tot = []
        for j in range(nsub):
            cols = slice(j * width, (j + 1) * width)
            ring(d, nz - 2, j).wait_recv()
            tot.append(val[:, cols] + rbuf[d, nz - 2, :, cols].astype(F32))
        tot = jnp.concatenate(tot, axis=1).astype(BF)
        for e in range(n):
            fin[d, e] = tot[2 * e : 2 * e + 2, :]
        for i, (ty, tx, t) in enumerate(others):
            q = remote(
                fin.at[d, t], out.at[c, me], fs.at[d, i], fr.at[c, me], (ty, tx, z, d)
            )
            q.start()
            sends.append(q)
    keep = remote(fin.at[1 - c, me], out.at[c, me], fs.at[0, n - 1], fr.at[c, me], sib)
    keep.start()
    sends.append(keep)
    out[c, me] = fin[c, me]
    for k in (0, 1):
        for ty, tx, t in others:
            remote(fin.at[0, t], out.at[k, t], fs.at[0, 0], fr.at[k, t], sib).wait_recv()
    remote(fin.at[0, me], out.at[1 - c, me], fs.at[0, 0], fr.at[1 - c, me], sib).wait_recv()
    for d, (ty, tx, t) in enumerate(others):
        remote(sent.at[t], inb.at[me], is_.at[d], ir.at[me], (ty, tx, z, c)).wait_send()
    wcopy.wait_send()
    for q in sends:
        q.wait_send()


def experts(sent, gate, up, down, ny, nx, nz, cid):
    n = ny * nx
    d_model, units = gate.shape
    half = d_model // 2
    per = 2 * n
    nsub = 2
    far = nz // 2
    dma = pltpu.SemaphoreType.DMA
    return pl.pallas_call(
        functools.partial(expert_kernel, ny, nx, nz, nsub),
        out_shape=jax.ShapeDtypeStruct((2, n, 2, half), BF),
        in_specs=[VM, ANY, ANY, ANY],
        out_specs=VM,
        scratch_shapes=[
            pltpu.VMEM((d_model, units), BF),
            pltpu.VMEM((d_model, units), BF),
            pltpu.VMEM((units, half), BF),
            pltpu.VMEM((units, half), BF),
            pltpu.VMEM((n, 2, d_model), BF),
            pltpu.VMEM((2 * nz, per, d_model), BF),
            pltpu.VMEM((2, 2 * nz, per, units), BF),
            pltpu.VMEM((2, nz - 1, per, half), BF),
            pltpu.VMEM((2, nz - 1, per, half), BF),
            pltpu.VMEM((2, n, 2, half), BF),
            dma((3,)),
            dma, dma,
            dma((n - 1,)), dma((n,)),
            dma((2, far + 1, 2)), dma((2, far + 1, 2)),
            dma((2, far + 1, 2)), dma((2, far + 1, 2)),
            dma((2 * nz,)), dma((2 * nz,)),
            dma((2, nz - 1, nsub)), dma((2, nz - 1, nsub)),
            dma((2, n)), dma((2, n)),
        ],
        compiler_params=pltpu.CompilerParams(
            collective_id=cid, has_side_effects=True, vmem_limit_bytes=LIMIT
        ),
        name="experts",
    )(sent, gate, up, down)


def normalize(rows, norm_gain):
    rows_f = rows.astype(F32)
    scaling = lax.rsqrt(jnp.mean(rows_f * rows_f, axis=1, keepdims=True) + 1e-06)
    return (rows_f * scaling * norm_gain[None, :]).astype(BF)


def route_weights(normed, group_router, expert_router, chosen, group_size):
    group_logits = dot(normed, group_router)
    expert_logits = dot(normed, expert_router)
    chosen_group = chosen[:, 0] // group_size
    margin = group_logits[:, 0] - group_logits[:, 1]
    own_margin = jnp.where(chosen_group == 0, margin, -margin)
    experts_iota = jnp.arange(expert_logits.shape[1], dtype=jnp.int32)
    picked = jnp.sum(
        jnp.where(
            chosen[:, :, None] == experts_iota[None, None, :], expert_logits[:, None, :], F32(0.0)
        ),
        axis=2,
    )
    return jax.nn.sigmoid(own_margin)[:, None] * jax.nn.sigmoid(picked - picked[:, ::-1])


def slot_table(chosen, expert_count, slots):
    flat_ids = chosen.reshape(-1)
    same = flat_ids[:, None] == flat_ids[None, :]
    at = jnp.arange(flat_ids.shape[0], dtype=jnp.int32)
    ranks = jnp.sum((same & (at[None, :] < at[:, None])).astype(jnp.int32), axis=1)
    return (flat_ids * slots + ranks).reshape(chosen.shape)


def per_device(
    residual_in, queries, keys, values, break_offset, doc_ids, out_weight, norm_gain,
    group_router, expert_router, expert_ids, gate_weight, up_weight, down_weight,
):
    ny, nx, nz = lax.axis_size("y"), lax.axis_size("x"), lax.axis_size("z")
    tok_dev = queries.shape[0]
    heads_dev = break_offset.shape[1]
    rows_dev, width = residual_in.shape
    experts_all = ny * nx
    own_begin = lax.axis_index(TP) * rows_dev
    aux = jnp.concatenate(
        [
            break_offset.T,
            doc_ids.astype(BF)[None, :],
            jnp.zeros((16 - heads_dev - 1, tok_dev), BF),
        ],
        axis=0,
    )
    kall, vall, aall, wsib = gather_keys(keys, values, aux, out_weight, ny, nx, 1)
    attended = attend(queries, kall, vall, aall, doc_ids.astype(F32)[:, None], nx)
    mixed_stream = project(attended, out_weight, wsib, residual_in, nz, 2)
    chosen = lax.dynamic_slice_in_dim(expert_ids, own_begin, rows_dev, 0)
    normed = normalize(mixed_stream, norm_gain)
    routes = route_weights(
        normed, group_router, expert_router, chosen, experts_all // GROUPS
    )
    slot_ids = slot_table(chosen, experts_all, 2)
    onehot = (
        jnp.arange(2 * experts_all, dtype=jnp.int32)[:, None, None] == slot_ids[None]
    ).sum(axis=2)
    sent = dot(onehot.astype(BF), normed).astype(BF).reshape(experts_all, 2, width)
    back = experts(sent, gate_weight[0], up_weight[0], down_weight[0], ny, nx, nz, 3)
    back = back.transpose(1, 2, 0, 3).reshape(2 * experts_all, width)
    expert_out = jnp.take(back, slot_ids.reshape(-1), axis=0).reshape(rows_dev, 2, width)
    mixture = jnp.sum(routes[:, :, None] * expert_out.astype(F32), axis=1)
    return (mixed_stream.astype(F32) + mixture).astype(BF)


def solution(mesh):
    n = mesh.shape["sp"]
    side = round(n**0.5)
    finer = Mesh(
        mesh.devices.reshape(side, n // side, mesh.shape["tp"] // 2, 2), AXES
    )
    in_specs = (
        P(SP + TP, None),
        P(SP, TP),
        P(SP, TP),
        P(SP, TP),
        P(SP, TP),
        P(SP),
        P(TP, None),
        P(),
        P(),
        P(),
        P(SP, None),
        P(SP, None, TP),
        P(SP, None, TP),
        P(SP, TP, None),
    )
    return jax.shard_map(
        per_device, mesh=finer, in_specs=in_specs, out_specs=P(SP + TP, None), check_vma=False
    )
```

time: 443 us -> 160 us (0.36); the launches traced: 437 us -> 159 us
  waiting for transfers between devices: 185 us -> 0 us
  Pallas kernels: 0 us -> 146 us
  other arithmetic: 97.7 us -> 5.22 us
  matrix products: 56.4 us -> 3.44 us
  blocking collectives: 31.9 us -> 0 us
  local copies, waits for them, and re-layouts: 34.8 us -> 4.72 us
  starting transfers between devices: 16.3 us -> 0 us
  between operations: 13.4 us -> 0.15 us
    pallas_call x0 -> x4, Pallas kernels: none -> 146 us  [the longest x1 83.9 us: experts(): pl.pallas_call(functools.partial(expert_kernel, ny, nx, nz, nsub), out_sh...]
    another operation x50 -> x0, other arithmetic: 77.2 us -> none
    all_gather x2 -> x0, waiting for transfers between devices: 72.5 us -> none  [the longest x1 38 us: per_device(): lax.all_gather(lax.all_to_all(sent, 'sp', split_axis=0, concat_axis=0, ti...]
    reduce_scatter x2 -> x0, waiting for transfers between devices: 57.1 us -> none  [the longest x1 40.7 us: summed_rows(): return lax.psum_scatter(blocks, chips, scatter_dimension=0, tiled=True)[0]]
    all_to_all x2 -> x0, waiting for transfers between devices: 55.3 us -> none  [the longest x1 48.1 us: summed_on_arrival(): lax.all_to_all(blocks, axis, split_axis=0, concat_axis=0, tiled=True)]
    dot_general x37 -> x3, matrix products: 56.4 us -> 3.44 us  [dot(): return jnp.dot(a, b, preferred_element_type=F32)]
    all_gather x1 -> x0, blocking collectives: 19.1 us -> none  [per_device(): lax.all_gather(doc_ids, 'sp', axis=0, tiled=True)]
    all_to_all x2 -> x0, starting transfers between devices: 15.9 us -> none  [the longest x1 9.41 us: summed_on_arrival(): lax.all_to_all(blocks, axis, split_axis=0, concat_axis=0, tiled=True)]
  transfers between devices with their start and end apart: 6 -> 0, of which waited for: 6 -> 0; matrix products, arithmetic and copies ran while one was open for 1% -> 0% of each run, Pallas kernels for 0% -> 0%
where the time goes in v1:
time: 160 us; the launch traced here: 159 us
  Pallas kernels  146 us (91%)
  other arithmetic  5.22 us (3%)
  local copies, waits for them, and re-layouts  4.72 us (3%)
  matrix products  3.44 us (2%)
    pallas_call x1, Pallas kernels, experts(): pl.pallas_call(functools.partial(expert_kernel, ny, nx, nz, nsub), out_sh...  83.9 us
    pallas_call x1, Pallas kernels, project(): pl.pallas_call(functools.partial(project_kernel, nz, nsub), out_shape=jax...  36 us
    pallas_call x1, Pallas kernels, gather_keys(): pl.pallas_call(functools.partial(gather_kernel, DOC_MOST // KB, ny, nx),...  22.3 us
    pallas_call x1, Pallas kernels, attend(): pl.pallas_call(functools.partial(attend_kernel, DOC_MOST // KB, nx), out_...  3.68 us
    dot_general x3, matrix products, dot(): return jnp.dot(a, b, preferred_element_type=F32)  3.44 us

profile of v1, /device:TPU:1, one launch (start us, length us, event | category | flops | bytes accessed | tf_op | source)
XLA Modules:
  0.0 159.4 jit_solution(15695922518442402618)
XLA Ops:
  0.0 0.0 copy-start
  0.0 0.8 fusion.14
  0.8 0.1 pad.2.clone
  0.8 1.3 maximum_maximum_fusion.a
  2.2 22.3 %gather_keys.1 = (bf16[16,256,128]{2,1,0:T(8,128)(2,1)}, bf16[16,256,128]{2,1,0:T(8,128)(2,1)}, bf16[16,16,256]{2,1,0:T(8,128)(2,1)}, bf16[128,2048]{1,0:T(8,128)(2,1)}) custom-call(bf16[256,128]{1,0:T(8,128)(2,1)} %k.1, bf16[256,128]{1,0:T(8,128)(2,1)} %v.1, bf16[16,256]{1,0:T(8,128)(2,1)} %maximum_maximum_fusion.a, bf16[128,4096]{1,0:T(8,128)(2,1)} %w.3), custom_call_target="tpu_custom_call" | custom-call | tf_op jit(solution)/shard_map/gather_keys/pallas_call | solution.py:152
  24.5 0.8 copy.29.qdoc
  25.3 0.0 copy-start.2
  25.3 0.0 copy-start.3
  25.3 0.0 copy-start.4
  25.3 3.7 %attend.1.att = bf16[256,128]{1,0:T(8,128)(2,1)} custom-call(bf16[256,128]{1,0:T(8,128)(2,1)} %q.1, bf16[16,256,128]{2,1,0:T(8,128)(2,1)} %get-tuple-element.9.k, bf16[16,256,128]{2,1,0:T(8,128)(2,1)} %get-tuple-element.10.v, bf16[16,16,256]{2,1,0:T(8,128)(2,1)} %get-tuple-element.11.a, f32[256,1]{1,0:T(8,128)} %copy.29.qdoc), custom_call_target="tpu_custom_call" | custom-call | tf_op jit(solution)/shard_map/attend/pallas_call | solution.py:219
  29.0 36.0 %project.1 = bf16[16,4096]{1,0:T(8,128)(2,1)} custom-call(bf16[256,128]{1,0:T(8,128)(2,1)} %attend.1.att, bf16[128,4096]{1,0:T(8,128)(2,1)} %w.3, bf16[128,2048]{1,0:T(8,128)(2,1)} %get-tuple-element.12.wsib, bf16[16,4096]{1,0:T(8,128)(2,1)} %res.1), custom_call_target="tpu_custom_call" | custom-call | tf_op jit(solution)/shard_map/project/pallas_call | solution.py:305
  65.0 1.1 fusion
  66.1 0.0 copy-done
  66.1 0.0 copy-done.2
  66.1 1.1 fusion.9
  67.2 0.0 copy-done.3
  67.2 0.1 broadcast_multiply_fusion
  67.3 0.2 select_reduce_fusion
  67.5 0.0 copy-done.4
  67.5 1.1 fusion.11
  68.7 0.1 copy.30
  68.7 0.1 copy.31
  68.8 0.1 reshape.71
  68.9 0.2 convert_reduce_fusion.1
  69.1 0.1 reduce_sum.52
  69.2 0.1 copy.32
  69.3 0.1 convert_reduce_fusion
  69.4 1.2 convolution_convert_fusion
  70.6 0.9 reshape.72.sent
  71.4 83.9 %experts.1 = bf16[2,16,2,2048]{3,2,1,0:T(2,128)(2,1)} custom-call(bf16[16,2,4096]{2,1,0:T(2,128)(2,1)} %reshape.72.sent, bf16[4096,256]{1,0:T(8,128)(2,1)} %bitcast.20, bf16[4096,256]{1,0:T(8,128)(2,1)} %bitcast.21, bf16[256,4096]{1,0:T(8,128)(2,1)} %bitcast.22), custom_call_target="tpu_custom_call" | custom-call | tf_op jit(solution)/shard_map/experts/pallas_call | solution.py:554
  155.3 1.2 copy.34
  156.6 0.0 copy-start.1
  156.6 0.1 copy.36
  156.7 0.1 copy.35
  156.8 0.1 mul.77
  156.9 0.7 gather_fusion
  157.6 0.2 gather.7
  157.8 0.1 copy.33
  157.9 0.8 multiply_reduce_fusion
  158.7 0.0 copy-done.1
  158.7 0.7 fusion.3
  (9 shorter events, 0.1 us)
Async XLA Ops:
  0.0 66.1 %copy-start = (bf16[4096,16]{0,1:T(8,128)(2,1)S(1)}, bf16[4096,16]{0,1:T(8,128)(2,1)}, u32[]{:S(2)}) copy-start(bf16[4096,16]{0,1:T(8,128)(2,1)} %param.23) | copy-start | bytes 393220
  25.3 40.8 %copy-start.2 = (f32[4096]{0:T(1024)S(1)}, f32[4096]{0:T(1024)}, u32[]{:S(2)}) copy-start(f32[4096]{0:T(1024)} %param.21) | copy-start | bytes 49156
  25.3 41.9 %copy-start.3 = (s32[256,2]{0,1:T(2,128)S(1)}, s32[256,2]{0,1:T(2,128)}, u32[]{:S(2)}) copy-start(s32[256,2]{0,1:T(2,128)} %param.24) | copy-start | bytes 6148
  25.3 42.2 %copy-start.4 = (bf16[4096,2]{0,1:T(2,128)(2,1)S(1)}, bf16[4096,2]{0,1:T(2,128)(2,1)}, u32[]{:S(2)}) copy-start(bf16[4096,2]{0,1:T(2,128)(2,1)} %param.22) | copy-start | bytes 49156
  156.6 2.1 %copy-start.1 = (bf16[16,4096]{1,0:T(8,128)(2,1)S(1)}, bf16[16,4096]{1,0:T(8,128)(2,1)}, u32[]{:S(2)}) copy-start(bf16[16,4096]{1,0:T(8,128)(2,1)} %project.1) | copy-start | bytes 393220

commit v2 on v0

v2 whole, which is shorter than its diff:
```python
import functools

import jax
import jax.numpy as jnp
from jax import lax
from jax.experimental import pallas as pl
from jax.experimental.pallas import tpu as pltpu
from jax.sharding import Mesh
from jax.sharding import PartitionSpec as P

HEAD_DIM = 64
GROUPS = 2
DOC_MOST = 2560
KB = 256
BAND = DOC_MOST // KB
NEG = -1e30
SUM_PIECES = 2
ROW_PIECES = 4
BACK_PIECES = 4
MESH = pl.DeviceIdType.MESH
AXES = ("y", "x", "z", "c")
SP = ("y", "x")
TP = ("z", "c")
VM = pl.BlockSpec(memory_space=pltpu.VMEM)
ANY = pl.BlockSpec(memory_space=pl.ANY)
BF = jnp.bfloat16
F32 = jnp.float32
LIMIT = 60 * 1024 * 1024


def dot(a, b):
    return jnp.dot(a, b, preferred_element_type=F32)


def dot_t(a, b):
    return lax.dot_general(a, b, (((1,), (1,)), ((), ())), preferred_element_type=F32)


def iota(shape, axis):
    return lax.broadcasted_iota(jnp.int32, shape, axis)


def remote(src, dst, ss, rs, to):
    return pltpu.make_async_remote_copy(
        src_ref=src, dst_ref=dst, send_sem=ss, recv_sem=rs, device_id=to, device_id_type=MESH
    )


def attend_block(diag, q, kb, vb, ab, qd, acc, st, later):
    heads = q.shape[1] // HEAD_DIM
    rows = q.shape[0]
    live = ab[heads : heads + 1, :].astype(F32) == qd[...]
    if diag:
        live = live & (iota((rows, KB), 1) < iota((rows, KB), 0))
    for h in range(heads):
        hs = slice(h * HEAD_DIM, (h + 1) * HEAD_DIM)
        s = dot_t(q[:, hs], kb[:, hs]) + ab[h : h + 1, :].astype(F32)
        s = jnp.where(live, s, NEG)
        go = jnp.maximum(s, 0.0) + jnp.log(1.0 + jnp.exp(-jnp.abs(s)))
        hi = go.astype(BF)
        lo = (go - hi.astype(F32)).astype(BF)
        within = dot(hi, later[...]) + dot(lo, later[...])
        wt = jnp.exp(s - go - within).astype(BF)
        o = dot(wt, vb[:, hs])
        total = jnp.sum(go, axis=1, keepdims=True)
        if diag:
            acc[:, hs] = o
            st[h] = total
        else:
            before = st[h]
            acc[:, hs] = acc[:, hs] + jnp.exp(-before) * o
            st[h] = before + total


def layer_kernel(
    dims,
    res, q, k, v, off, doc, w, gain, grp, exr, ids, gate, up, down,
    out,
    kall, vall, aall, auxo, later, qs, qd, acc, st,
    wown, wsib, att, pair, part, sbb, rbb, xbuf, ybuf, mixed,
    sent, inb, rows, gw, uw, dw, dsib, hid, partc, sbc, rbc, fin, ret, back, grw, exw,
    lsem, ks, kr, vs, vr, as_, ar, ws, wr, ds, dr, bs, br, es, er,
    is_, ir, gs, gr, cs, cr, hs_, hr_, ss, rs, fs, fr,
):
    ny, nx, nz = dims
    y, x, z, c = (lax.axis_index(a) for a in AXES)
    me = y * nx + x
    n = ny * nx
    sib = (y, x, z, 1 - c)
    right = (y, x, lax.rem(z + 1, nz), c)
    left = (y, x, lax.rem(z + nz - 1, nz), c)
    half = wown.shape[1]
    heads = off.shape[1]
    own_half = pl.ds(pl.multiple_of(c * half, half), half)
    other_half = pl.ds(pl.multiple_of((1 - c) * half, half), half)
    far = nz // 2
    sends = []

    def start(q_):
        q_.start()
        sends.append(q_)

    loads = [
        pltpu.make_async_copy(w.at[:, own_half], wown, lsem.at[0]),
        pltpu.make_async_copy(gate, gw, lsem.at[1]),
        pltpu.make_async_copy(up, uw, lsem.at[2]),
        pltpu.make_async_copy(down.at[:, own_half], dw, lsem.at[3]),
        pltpu.make_async_copy(grp, grw, lsem.at[4]),
        pltpu.make_async_copy(exr, exw, lsem.at[5]),
    ]
    for a in loads:
        a.start()
    others = []
    for d in range(1, n):
        t = lax.rem(me + d, n)
        others.append((lax.div(t, nx), lax.rem(t, nx), t))
    peers = [(ty, tx, z, c) for ty, tx, t in others]
    peers += [(ty, tx, z, 1 - c) for ty, tx, t in others]
    peers += [right, left, sib]
    bar = pltpu.get_barrier_semaphore()
    for p in peers:
        pl.semaphore_signal(bar, inc=1, device_id=p, device_id_type=MESH)

    eye = (iota((KB, KB), 0) == iota((KB, KB), 1)).astype(BF)
    later[...] = (iota((KB, KB), 0) > iota((KB, KB), 1)).astype(BF)
    docf = doc[...].astype(F32)
    qd[...] = jnp.sum(jnp.where(eye > 0, docf, 0.0), axis=1, keepdims=True)
    offs = []
    for h in range(heads):
        col = off[:, h : h + 1].astype(F32)
        offs.append(jnp.sum(jnp.where(eye > 0, col, 0.0), axis=0, keepdims=True))
    pad = jnp.zeros((auxo.shape[0] - heads - 1, KB), F32)
    auxo[...] = jnp.concatenate(offs + [docf, pad], axis=0).astype(BF)
    qs[...] = q[...] * BF(HEAD_DIM**-0.5)
    pl.semaphore_wait(bar, len(peers))

    xs = [lax.rem(x + d, nx) for d in range(1, nx)]
    ys = [lax.rem(y + d, ny) for d in range(1, ny)]
    xb = [lax.rem(x + nx - d, nx) for d in range(1, nx)]
    yb = [lax.rem(y + ny - d, ny) for d in range(1, ny)]

    def used(b, j):
        return (j > b) & (j - b <= BAND)

    def k_first(src, dst):
        return (dst > src) | (y < ny - 1)

    def v_first(dst, src, col):
        return (dst > src) & (nx * (dst - src) - col <= BAND)

    def kcopy(b, src, asrc, i, to):
        return (
            remote(src, kall.at[b], ks.at[i], kr.at[b], to),
            remote(asrc, aall.at[b], as_.at[i], ar.at[b], to),
        )

    def vcopy(b, src, i, to):
        return (remote(src, vall.at[b], vs.at[i], vr.at[b], to),)

    plan = []

    def send(cond, copies):
        plan.append((cond, copies))

        @pl.when(cond)
        def _():
            for a in copies:
                a.start()

    def arrive(cond, copies):
        @pl.when(cond)
        def _():
            for a in copies:
                a.wait_recv()

    nk = nv = 0
    for a in xs:
        send(k_first(x, a), kcopy(me, k, auxo, nk, (y, a, z, c)))
        nk += 1
    for a in ys:
        send(v_first(a, y, x), vcopy(me, v, nv, (a, x, z, c)))
        nv += 1
    for a in ys:
        send(used(me, a * nx + x), kcopy(me, k, auxo, nk, (a, x, z, c)))
        nk += 1
    for a in xs:
        send(used(me, y * nx + a), vcopy(me, v, nv, (y, a, z, c)))
        nv += 1
    start(remote(w.at[:, other_half], wsib, ws.at[0], wr.at[0], sib))
    start(remote(down.at[:, other_half], dsib, ws.at[1], wr.at[1], sib))

    attend_block(True, qs, k, v, auxo, qd, acc, st, later)

    firsts = []
    for i in range(max(nx, ny) - 1):
        if i < nx - 1:
            b = y * nx + xb[i]
            got = k_first(xb[i], x)
            arrive(got, kcopy(b, k, auxo, 0, sib))
            for a in ys:
                send(got & used(b, a * nx + x), kcopy(b, kall.at[b], aall.at[b], nk, (a, x, z, c)))
                nk += 1
        if i < ny - 1:
            b = yb[i] * nx + x
            got = v_first(y, yb[i], x)
            arrive(got, vcopy(b, v, 0, sib))
            for a in xs:
                send(got & used(b, y * nx + a), vcopy(b, vall.at[b], nv, (y, a, z, c)))
                nv += 1
    del firsts

    def step(t, carry):
        b = me - t
        by = lax.div(b, nx)
        bx = lax.rem(b, nx)

        @pl.when(by != y)
        def _():
            for a in kcopy(b, k, auxo, 0, sib):
                a.wait_recv()

        @pl.when(bx != x)
        def _():
            for a in vcopy(b, v, 0, sib):
                a.wait_recv()

        attend_block(
            False, qs, kall.at[b], vall.at[b], aall.at[b], qd, acc, st, later
        )
        return carry

    lax.fori_loop(1, jnp.minimum(me, BAND) + 1, step, 0)
    att[...] = acc[...].astype(BF)
    swap = remote(att, pair, ds, dr, sib)
    start(swap)

    def ring_sum(own, sbuf, rbuf, s_sem, r_sem, np_, hr, last):
        def move(d, s, p):
            ref = (d, s, pl.ds(p * hr, hr))
            return remote(
                sbuf.at[ref], rbuf.at[ref], s_sem.at[d, s, p], r_sem.at[d, s, p],
                right if d == 0 else left,
            )

        def half_of(d):
            return range(np_ // 2) if d == 0 else range(np_ // 2, np_)

        for s in range(far):
            for i in range(np_ // 2 if s == 0 else np_):
                for d in range(2):
                    order = list(half_of(d)) + ([] if s == 0 else list(half_of(1 - d)))
                    p = order[i]
                    dist = far - s
                    zz = lax.rem(z + dist, nz) if d == 0 else lax.rem(z + nz - dist, nz)
                    val = own(zz, p)
                    if s > 1 or (s == 1 and p in half_of(d)):
                        move(d, s - 1, p).wait_recv()
                        val = val + rbuf[d, s - 1, p * hr : (p + 1) * hr, :].astype(F32)
                    sbuf[d, s, p * hr : (p + 1) * hr, :] = val.astype(BF)
                    start(move(d, s, p))
        for i in range(np_):
            p = i
            for d in range(2):
                move(d, far - 1, p).wait_recv()
            tot = own(z, p)
            for d in range(2):
                tot = tot + rbuf[d, far - 1, p * hr : (p + 1) * hr, :].astype(F32)
            last(p, tot)

    chunk = part.shape[0] // nz
    hr = chunk // SUM_PIECES
    loads[0].wait()
    part[...] = dot(att[...], wown[...])
    remote(w.at[:, other_half], wsib, ws.at[0], wr.at[0], sib).wait_recv()
    swap.wait_recv()
    part[...] += dot(pair[...], wsib[...])

    def own_b(zz, p):
        return part[pl.ds(pl.multiple_of(zz * chunk + p * hr, hr), hr), :]

    crow = chunk // 2

    def last_b(p, tot):
        for i in range(max(1, hr // crow)):
            r = p * hr + i * crow if hr >= crow else p * hr
            cnt = min(hr, crow)
            core = r // crow
            at = r % crow
            piece = tot[i * crow : i * crow + cnt] if hr >= crow else tot

            @pl.when(c == core)
            def _():
                ybuf[c, at : at + cnt, :] = piece

            @pl.when(c != core)
            def _():
                xbuf[at : at + cnt, :] = piece

    ring_sum(own_b, sbb, rbb, bs, br, SUM_PIECES, hr, last_b)
    trade = remote(xbuf, ybuf.at[c], es, er, sib)
    start(trade)
    remote(xbuf, ybuf.at[1 - c], es, er, sib).wait_recv()
    lo = res[:, :half].astype(F32) + ybuf[0]
    hi = res[:, half:].astype(F32) + ybuf[1]
    mlo, mhi = lo.astype(BF), hi.astype(BF)
    mixed[:, :half] = mlo
    mixed[:, half:] = mhi
    lo, hi = mlo.astype(F32), mhi.astype(F32)
    mean = (
        jnp.sum(lo * lo, axis=1, keepdims=True) + jnp.sum(hi * hi, axis=1, keepdims=True)
    ) / (2 * half)
    scale = lax.rsqrt(mean + 1e-06)
    nlo = (lo * scale * gain[:, :half]).astype(BF)
    nhi = (hi * scale * gain[:, half:]).astype(BF)

    tok = res.shape[0]
    chosen = ids[pl.ds(pl.multiple_of((z * 2 + c) * tok, tok), tok), :]
    eye16 = iota((tok, tok), 0) == iota((tok, tok), 1)
    trow = [
        jnp.sum(jnp.where(eye16, chosen[:, i : i + 1], 0), axis=0, keepdims=True)
        for i in range(2)
    ]
    slot = iota((2 * n, tok), 0)
    expert_of = lax.div(slot, 2)
    named = ((trow[0] == expert_of) | (trow[1] == expert_of)).astype(F32)
    earlier = (iota((tok, tok), 0) < iota((tok, tok), 1)).astype(BF)
    rank = dot(named.astype(BF), earlier)
    odd = lax.rem(slot, 2).astype(F32)
    pick = jnp.where(rank == odd, named, 0.0).astype(BF)
    slo = dot(pick, nlo).astype(BF)
    shi = dot(pick, nhi).astype(BF)
    for e in range(n):
        sent[e, :, :half] = slo[2 * e : 2 * e + 2, :]
        sent[e, :, half:] = shi[2 * e : 2 * e + 2, :]

    for d, (ty, tx, t) in enumerate(others):
        start(remote(sent.at[t], inb.at[me], is_.at[d], ir.at[me], (ty, tx, z, c)))
    inb[me] = sent[me]

    normed = jnp.concatenate([nlo, nhi], axis=1)
    loads[4].wait()
    loads[5].wait()
    glog = dot(normed, grw[...])
    elog = dot(normed, exw[...])
    margin = glog[:, 0:1] - glog[:, 1:2]
    own_margin = jnp.where(chosen[:, 0:1] < n // GROUPS, margin, -margin)
    share = jax.nn.sigmoid(own_margin)
    eid = iota((tok, n), 1)
    picked = [
        jnp.sum(jnp.where(chosen[:, i : i + 1] == eid, elog, 0.0), axis=1, keepdims=True)
        for i in range(2)
    ]
    route = [share * jax.nn.sigmoid(picked[i] - picked[1 - i]) for i in range(2)]
    slot_c = iota((tok, 2 * n), 1)
    exp_c = lax.div(slot_c, 2)
    is_k = [chosen[:, i : i + 1] == exp_c for i in range(2)]
    named_c = (is_k[0] | is_k[1]).astype(BF)
    before = (iota((tok, tok), 1) < iota((tok, tok), 0)).astype(BF)
    rank_c = dot(before, named_c)
    odd_c = lax.rem(slot_c, 2).astype(F32)
    take = [
        jnp.where(is_k[i] & (rank_c == odd_c), 1.0, 0.0).astype(BF) for i in range(2)
    ]

    for ty, tx, t in others:
        remote(sent.at[t], inb.at[t], is_.at[0], ir.at[t], sib).wait_recv()
    mine = z * 2 + c
    for e in range(n):
        rows[mine, 2 * e : 2 * e + 2, :] = inb[e]

    per = rows.shape[1]
    hb = per // ROW_PIECES

    def piece(b, p):
        return rows.at[b, pl.ds(p * hb, hb), :]

    def from_chip(d, h):
        return lax.rem(z + nz - h, nz) if d == 0 else lax.rem(z + h, nz)

    def hop(d, h, p):
        b = from_chip(d, h - 1) * 2 + c
        return remote(
            piece(b, p), piece(b, p), gs.at[d, h, p], gr.at[d, h, p], right if d == 0 else left
        )

    def got_hop(d, h, p):
        b = from_chip(d, h) * 2 + c
        return remote(piece(b, p), piece(b, p), gs.at[d, h, p], gr.at[d, h, p], sib)

    def cross(d, h, p, core):
        b = from_chip(d, h) * 2 + core
        return remote(piece(b, p), piece(b, p), cs.at[d, h, p], cr.at[d, h, p], sib)

    def pieces(d, h):
        if h < far:
            return list(range(ROW_PIECES))
        hp = ROW_PIECES // 2
        return list(range(hp)) if d == 0 else list(range(hp, ROW_PIECES))

    def order(d):
        hp = ROW_PIECES // 2
        a = list(range(hp))
        b = list(range(hp, ROW_PIECES))
        return a + b if d == 0 else b + a

    for i in range(ROW_PIECES):
        for d in (0, 1):
            start(hop(d, 1, order(d)[i]))
    for p in range(ROW_PIECES):
        start(cross(0, 0, p, c))

    def blocks_of(h):
        if h == 0:
            return [(z * 2 + i, i) for i in (0, 1)]
        lo_ = from_chip(0, h)
        hi_ = from_chip(1, h)
        if h == far:
            return [(lo_ * 2 + i, 4 * h - 2 + i) for i in (0, 1)]
        return [(lo_ * 2 + i, 4 * h - 2 + i) for i in (0, 1)] + [
            (hi_ * 2 + i, 4 * h + i) for i in (0, 1)
        ]

    def hswap(b, i):
        return remote(hid.at[0, b], hid.at[1, b], hs_.at[i], hr_.at[i], sib)

    def run(h):
        for d in (0, 1):
            if h == 0 and d == 1:
                continue
            for p in pieces(d, h):
                cross(d, h, p, 1 - c).wait_recv()
        bl = blocks_of(h)
        xin = jnp.concatenate([rows[b] for b, i in bl], axis=0)
        g = dot(xin, gw[...])
        u = dot(xin, uw[...])
        hv = (g * jax.nn.sigmoid(g) * u).astype(BF)
        for j, (b, i) in enumerate(bl):
            hid[0, b] = hv[j * per : (j + 1) * per]
            start(hswap(b, i))

    def finish(h):
        bl = blocks_of(h)
        for b, i in bl:
            hswap(b, i).wait_recv()
        h0 = jnp.concatenate([hid[0, b] for b, i in bl], axis=0)
        h1 = jnp.concatenate([hid[1, b] for b, i in bl], axis=0)
        val = dot(h0, dw[...]) + dot(h1, dsib[...])
        for j, (b, i) in enumerate(bl):
            partc[b] = val[j * per : (j + 1) * per]

    loads[1].wait()
    loads[2].wait()
    for h in range(1, far + 1):
        for i in range(ROW_PIECES):
            for d in (0, 1):
                p = order(d)[i]
                if p not in pieces(d, h):
                    continue
                got_hop(d, h, p).wait_recv()
                if h + 1 <= far and p in pieces(d, h + 1):
                    start(hop(d, h + 1, p))
                start(cross(d, h, p, c))
            if i == 0:
                run(h - 1)
                if h == 1:
                    loads[3].wait()
                    remote(down.at[:, other_half], dsib, ws.at[1], wr.at[1], sib).wait_recv()
            if i == 1:
                finish(h - 1)
    run(far)
    finish(far)

    chunk_c = 2 * per
    hc = chunk_c // BACK_PIECES

    def own_c(zz, p):
        b = zz * 2 + (p * hc) // per
        return partc[b, (p * hc) % per : (p * hc) % per + hc, :]

    def last_c(p, tot):
        core = (p * hc) // per
        e0 = ((p * hc) % per) // 2
        tb = tot.astype(BF)
        for e in range(hc // 2):
            t = e0 + e
            fin[core, t] = tb[2 * e : 2 * e + 2, :]
            ty, tx = t // nx, t % nx

            @pl.when(me != t)
            def _(t=t, ty=ty, tx=tx):
                remote(
                    fin.at[core, t], ret.at[c, me], fs.at[core, t], fr.at[c, me], (ty, tx, z, core)
                ).start()

            @pl.when((me == t) & (c != core))
            def _(t=t):
                remote(
                    fin.at[core, t], ret.at[c, me], fs.at[core, t], fr.at[c, me], sib
                ).start()

    ring_sum(own_c, sbc, rbc, ss, rs, BACK_PIECES, hc, last_c)
    ret[c, me] = fin[c, me]
    for i in (0, 1):
        for t in range(n):

            @pl.when((me != t) | (c != i))
            def _(t=t, i=i):
                remote(fin.at[0, t], ret.at[i, t], fs.at[0, t], fr.at[i, t], sib).wait_recv()

            back[2 * t : 2 * t + 2, i * half : (i + 1) * half] = ret[i, t]
    for i in range(2):
        cols = slice(i * half, (i + 1) * half)
        bk = back[:, cols]
        mix = route[0] * dot(take[0], bk) + route[1] * dot(take[1], bk)
        out[:, cols] = (mixed[:, cols].astype(F32) + mix).astype(BF)

    for cond, copies in plan:

        @pl.when(cond)
        def _(copies=copies):
            for a in copies:
                a.wait_send()

    for core in (0, 1):
        for t in range(n):

            @pl.when((me != t) | (c != core))
            def _(t=t, core=core):
                remote(
                    fin.at[core, t], ret.at[c, me], fs.at[core, t], fr.at[c, me], sib
                ).wait_send()

    for a in sends:
        a.wait_send()


def per_device(
    residual_in, queries, keys, values, break_offset, doc_ids, out_weight, norm_gain,
    group_router, expert_router, expert_ids, gate_weight, up_weight, down_weight,
):
    ny, nx, nz = lax.axis_size("y"), lax.axis_size("x"), lax.axis_size("z")
    n = ny * nx
    rows, att = queries.shape
    tok, width = residual_in.shape
    half = width // 2
    heads = break_offset.shape[1]
    gate, up, down = gate_weight[0], up_weight[0], down_weight[0]
    units = gate.shape[1]
    per = 2 * n
    far = nz // 2
    sends = (nx - 1) + (ny - 1) + (nx - 1) * (ny - 1)
    dma = pltpu.SemaphoreType.DMA
    vm = pltpu.VMEM
    scratch = [
        vm((n, rows, att), BF), vm((n, rows, att), BF), vm((n, 16, rows), BF), vm((16, rows), BF),
        vm((KB, KB), BF), vm((rows, att), BF), vm((rows, 1), F32), vm((rows, att), F32),
        vm((heads, rows, 1), F32),
        vm((att, half), BF), vm((att, half), BF), vm((rows, att), BF), vm((rows, att), BF),
        vm((rows, half), F32),
        vm((2, far, rows // nz, half), BF), vm((2, far, rows // nz, half), BF),
        vm((tok, half), F32), vm((2, tok, half), F32), vm((tok, width), BF),
        vm((n, 2, width), BF), vm((n, 2, width), BF), vm((2 * nz, per, width), BF),
        vm((width, units), BF), vm((width, units), BF), vm((units, half), BF),
        vm((units, half), BF),
        vm((2, 2 * nz, per, units), BF), vm((2 * nz, per, half), F32),
        vm((2, far, 2 * per, half), BF), vm((2, far, 2 * per, half), BF),
        vm((2, n, 2, half), BF), vm((2, n, 2, half), BF), vm((per, width), BF),
        vm(group_router.shape, BF), vm(expert_router.shape, BF),
        dma((6,)),
        dma((sends,)), dma((n,)), dma((sends,)), dma((n,)), dma((sends,)), dma((n,)),
        dma((2,)), dma((2,)), dma, dma,
        dma((2, far, SUM_PIECES)), dma((2, far, SUM_PIECES)), dma, dma,
        dma((n - 1,)), dma((n,)),
        dma((2, far + 1, ROW_PIECES)), dma((2, far + 1, ROW_PIECES)),
        dma((2, far + 1, ROW_PIECES)), dma((2, far + 1, ROW_PIECES)),
        dma((2 * nz,)), dma((2 * nz,)),
        dma((2, far, BACK_PIECES)), dma((2, far, BACK_PIECES)),
        dma((2, n)), dma((2, n)),
    ]
    return pl.pallas_call(
        functools.partial(layer_kernel, (ny, nx, nz)),
        out_shape=jax.ShapeDtypeStruct(residual_in.shape, BF),
        in_specs=[VM] * 6 + [ANY, VM, ANY, ANY, VM, ANY, ANY, ANY],
        out_specs=VM,
        scratch_shapes=scratch,
        compiler_params=pltpu.CompilerParams(
            collective_id=1, has_side_effects=True, vmem_limit_bytes=LIMIT
        ),
        name="layer",
    )(
        residual_in, queries, keys, values, break_offset, doc_ids[None, :], out_weight,
        norm_gain[None, :], group_router, expert_router, expert_ids, gate, up, down,
    )


def solution(mesh):
    n = mesh.shape["sp"]
    side = round(n**0.5)
    finer = Mesh(mesh.devices.reshape(side, n // side, mesh.shape["tp"] // 2, 2), AXES)
    in_specs = (
        P(SP + TP, None),
        P(SP, TP),
        P(SP, TP),
        P(SP, TP),
        P(SP, TP),
        P(SP),
        P(TP, None),
        P(),
        P(),
        P(),
        P(SP, None),
        P(SP, None, TP),
        P(SP, None, TP),
        P(SP, TP, None),
    )
    return jax.shard_map(
        per_device, mesh=finer, in_specs=in_specs, out_specs=P(SP + TP, None), check_vma=False
    )
```

time: 443 us -> 128 us (0.29); the launches traced: 437 us -> 127 us
  waiting for transfers between devices: 185 us -> 0 us
  Pallas kernels: 0 us -> 118 us
  other arithmetic: 97.7 us -> 0 us
  matrix products: 56.4 us -> 0 us
  blocking collectives: 31.9 us -> 0 us
  local copies, waits for them, and re-layouts: 34.8 us -> 8.86 us
  starting transfers between devices: 16.3 us -> 0 us
  between operations: 13.4 us -> 0.01 us
    pallas_call x0 -> x1, Pallas kernels: none -> 118 us  [per_device(): pl.pallas_call(functools.partial(layer_kernel, (ny, nx, nz)), out_shape=j...]
    another operation x50 -> x0, other arithmetic: 77.2 us -> none
    all_gather x2 -> x0, waiting for transfers between devices: 72.5 us -> none  [the longest x1 38 us: per_device(): lax.all_gather(lax.all_to_all(sent, 'sp', split_axis=0, concat_axis=0, ti...]
    reduce_scatter x2 -> x0, waiting for transfers between devices: 57.1 us -> none  [the longest x1 40.7 us: summed_rows(): return lax.psum_scatter(blocks, chips, scatter_dimension=0, tiled=True)[0]]
    dot_general x37 -> x0, matrix products: 56.4 us -> none  [the longest x16 22.9 us: block_result(): jnp.einsum('qhd,khd->hqk', query_heads, key_block, preferred_element_type...]
    all_to_all x2 -> x0, waiting for transfers between devices: 55.3 us -> none  [the longest x1 48.1 us: summed_on_arrival(): lax.all_to_all(blocks, axis, split_axis=0, concat_axis=0, tiled=True)]
    all_gather x1 -> x0, blocking collectives: 19.1 us -> none  [per_device(): lax.all_gather(doc_ids, 'sp', axis=0, tiled=True)]
    all_to_all x2 -> x0, starting transfers between devices: 15.9 us -> none  [the longest x1 9.41 us: summed_on_arrival(): lax.all_to_all(blocks, axis, split_axis=0, concat_axis=0, tiled=True)]
  transfers between devices with their start and end apart: 6 -> 0, of which waited for: 6 -> 0; matrix products, arithmetic and copies ran while one was open for 1% -> 0% of each run, Pallas kernels for 0% -> 0%
where the time goes in v2:
time: 128 us; the launch traced here: 127 us
  Pallas kernels  118 us (92%)
  local copies, waits for them, and re-layouts  8.86 us (7%)
    pallas_call x1, Pallas kernels, per_device(): pl.pallas_call(functools.partial(layer_kernel, (ny, nx, nz)), out_shape=j...  118 us
    unnamed x5, local copies, waits for them, and re-layouts  8.86 us

profile of v2, /device:TPU:1, one launch (start us, length us, event | category | flops | bytes accessed | tf_op | source)
XLA Modules:
  0.0 127.3 jit_solution(15183888334955358301)
XLA Ops:
  0.0 1.4 %copy.15.off = bf16[256,2]{1,0:T(8,128)(2,1)} copy(bf16[256,2]{0,1:T(2,128)(2,1)} %param.18) | data formatting | bytes 2048 | tf_op args[4]
  1.4 1.5 %copy.18.ids = s32[256,2]{1,0:T(8,128)} copy(s32[256,2]{0,1:T(2,128)} %param.24) | data formatting | bytes 4096 | tf_op args[10]
  2.9 2.1 %copy.16.grp = bf16[4096,2]{1,0:T(8,128)(2,1)} copy(bf16[4096,2]{0,1:T(2,128)(2,1)} %param.22) | data formatting | bytes 32768 | tf_op args[8]
  5.0 2.3 %copy.17.exr = bf16[4096,16]{1,0:T(8,128)(2,1)} copy(bf16[4096,16]{0,1:T(8,128)(2,1)} %param.23) | data formatting | bytes 262144 | tf_op args[9]
  7.3 118.4 %layer.1 = bf16[16,4096]{1,0:T(8,128)(2,1)} custom-call(bf16[16,4096]{1,0:T(8,128)(2,1)} %res.1, bf16[256,128]{1,0:T(8,128)(2,1)} %q.1, bf16[256,128]{1,0:T(8,128)(2,1)} %k.1, bf16[256,128]{1,0:T(8,128)(2,1)} %v.1, bf16[256,2]{1,0:T(8,128)(2,1)} %copy.15.off, s32[1,256]{1,0:T(1,128)} %bitcast.9, bf16[128,4096]{1,0:T(8,128)(2,1)} %w.1, f32[1,4096]{1,0:T(1,128)} %bitcast.8, ...), custom_call_target="tpu_custom_call" | custom-call | tf_op jit(solution)/shard_map/layer/pallas_call | solution.py:580
  125.7 1.6 %copy.20 = bf16[16,4096]{1,0:T(8,128)(2,1)} copy(bf16[16,4096]{1,0:T(8,128)(2,1)} %layer.1) | data formatting | bytes 262144

commit v3 on v2

--- a/solution.py
+++ b/solution.py
@@ -47,35 +47,37 @@
 
 
 def attend_block(diag, q, kb, vb, ab, qd, acc, st, later):
-    heads = q.shape[1] // HEAD_DIM
+    heads = range(q.shape[1] // HEAD_DIM)
     rows = q.shape[0]
-    live = ab[heads : heads + 1, :].astype(F32) == qd[...]
+    cols = [slice(h * HEAD_DIM, (h + 1) * HEAD_DIM) for h in heads]
+    scores = [dot_t(q[:, cols[h]], kb[:, cols[h]]) for h in heads]
+    live = ab[len(heads) : len(heads) + 1, :].astype(F32) == qd[...]
     if diag:
         live = live & (iota((rows, KB), 1) < iota((rows, KB), 0))
-    for h in range(heads):
-        hs = slice(h * HEAD_DIM, (h + 1) * HEAD_DIM)
-        s = dot_t(q[:, hs], kb[:, hs]) + ab[h : h + 1, :].astype(F32)
-        s = jnp.where(live, s, NEG)
+    log_w, total = [], []
+    for h in heads:
+        s = jnp.where(live, scores[h] + ab[h : h + 1, :].astype(F32), NEG)
         go = jnp.maximum(s, 0.0) + jnp.log(1.0 + jnp.exp(-jnp.abs(s)))
         hi = go.astype(BF)
         lo = (go - hi.astype(F32)).astype(BF)
-        within = dot(hi, later[...]) + dot(lo, later[...])
-        wt = jnp.exp(s - go - within).astype(BF)
-        o = dot(wt, vb[:, hs])
-        total = jnp.sum(go, axis=1, keepdims=True)
+        total.append(jnp.sum(go, axis=1, keepdims=True))
+        log_w.append((s - go, dot(hi, later[...]) + dot(lo, later[...])))
+    for h in heads:
+        o = dot(jnp.exp(log_w[h][0] - log_w[h][1]).astype(BF), vb[:, cols[h]])
         if diag:
-            acc[:, hs] = o
-            st[h] = total
+            acc[:, cols[h]] = o
+            st[h] = total[h]
         else:
             before = st[h]
-            acc[:, hs] = acc[:, hs] + jnp.exp(-before) * o
-            st[h] = before + total
+            acc[:, cols[h]] = acc[:, cols[h]] + jnp.exp(-before) * o
+            st[h] = before + total[h]
 
 
 def layer_kernel(
     dims,
-    res, q, k, v, off, doc, w, gain, grp, exr, ids, gate, up, down,
+    res_, q_, k_, v_, off_, doc_, w, gain_, grp, exr, ids_, gate, up, down,
     out,
+    res, q, k, v, off, doc, gain, ids,
     kall, vall, aall, auxo, later, qs, qd, acc, st,
     wown, wsib, att, pair, part, sbb, rbb, xbuf, ybuf, mixed,
     sent, inb, rows, gw, uw, dw, dsib, hid, partc, sbc, rbc, fin, ret, back, grw, exw,
@@ -90,7 +92,7 @@
     right = (y, x, lax.rem(z + 1, nz), c)
     left = (y, x, lax.rem(z + nz - 1, nz), c)
     half = wown.shape[1]
-    heads = off.shape[1]
+    heads = off.shape[0]
     own_half = pl.ds(pl.multiple_of(c * half, half), half)
     other_half = pl.ds(pl.multiple_of((1 - c) * half, half), half)
     far = nz // 2
@@ -100,16 +102,6 @@
         q_.start()
         sends.append(q_)
 
-    loads = [
-        pltpu.make_async_copy(w.at[:, own_half], wown, lsem.at[0]),
-        pltpu.make_async_copy(gate, gw, lsem.at[1]),
-        pltpu.make_async_copy(up, uw, lsem.at[2]),
-        pltpu.make_async_copy(down.at[:, own_half], dw, lsem.at[3]),
-        pltpu.make_async_copy(grp, grw, lsem.at[4]),
-        pltpu.make_async_copy(exr, exw, lsem.at[5]),
-    ]
-    for a in loads:
-        a.start()
     others = []
     for d in range(1, n):
         t = lax.rem(me + d, n)
@@ -120,17 +112,31 @@
     bar = pltpu.get_barrier_semaphore()
     for p in peers:
         pl.semaphore_signal(bar, inc=1, device_id=p, device_id_type=MESH)
-
-    eye = (iota((KB, KB), 0) == iota((KB, KB), 1)).astype(BF)
+    small = [
+        pltpu.make_async_copy(a, b, lsem.at[6 + i])
+        for i, (a, b) in enumerate(
+            [(off_, off), (doc_, doc), (k_, k), (v_, v), (q_, q), (ids_, ids), (gain_, gain), (res_, res)]
+        )
+    ]
+    loads = [
+        pltpu.make_async_copy(w.at[:, own_half], wown, lsem.at[0]),
+        pltpu.make_async_copy(gate, gw, lsem.at[1]),
+        pltpu.make_async_copy(up, uw, lsem.at[2]),
+        pltpu.make_async_copy(down.at[:, own_half], dw, lsem.at[3]),
+        pltpu.make_async_copy(grp, grw, lsem.at[4]),
+        pltpu.make_async_copy(exr, exw, lsem.at[5]),
+    ]
+    for a in small + loads:
+        a.start()
+
     later[...] = (iota((KB, KB), 0) > iota((KB, KB), 1)).astype(BF)
+    for a in small:
+        a.wait()
     docf = doc[...].astype(F32)
-    qd[...] = jnp.sum(jnp.where(eye > 0, docf, 0.0), axis=1, keepdims=True)
-    offs = []
-    for h in range(heads):
-        col = off[:, h : h + 1].astype(F32)
-        offs.append(jnp.sum(jnp.where(eye > 0, col, 0.0), axis=0, keepdims=True))
+    eye = iota((KB, KB), 0) == iota((KB, KB), 1)
+    qd[...] = jnp.sum(jnp.where(eye, docf, 0.0), axis=1, keepdims=True)
     pad = jnp.zeros((auxo.shape[0] - heads - 1, KB), F32)
-    auxo[...] = jnp.concatenate(offs + [docf, pad], axis=0).astype(BF)
+    auxo[...] = jnp.concatenate([off[...].astype(F32), docf, pad], axis=0).astype(BF)
     qs[...] = q[...] * BF(HEAD_DIM**-0.5)
     pl.semaphore_wait(bar, len(peers))
 
@@ -314,10 +320,13 @@
     nhi = (hi * scale * gain[:, half:]).astype(BF)
 
     tok = res.shape[0]
-    chosen = ids[pl.ds(pl.multiple_of((z * 2 + c) * tok, tok), tok), :]
+    here = iota((tok, KB), 1) == (z * 2 + c) * tok + iota((tok, KB), 0)
+    chosen = [
+        jnp.sum(jnp.where(here, ids[i : i + 1, :], 0), axis=1, keepdims=True) for i in range(2)
+    ]
     eye16 = iota((tok, tok), 0) == iota((tok, tok), 1)
     trow = [
-        jnp.sum(jnp.where(eye16, chosen[:, i : i + 1], 0), axis=0, keepdims=True)
+        jnp.sum(jnp.where(eye16, chosen[i], 0), axis=0, keepdims=True)
         for i in range(2)
     ]
     slot = iota((2 * n, tok), 0)
@@ -340,20 +349,20 @@
     normed = jnp.concatenate([nlo, nhi], axis=1)
     loads[4].wait()
     loads[5].wait()
-    glog = dot(normed, grw[...])
-    elog = dot(normed, exw[...])
+    glog = dot_t(normed, grw[...])
+    elog = dot_t(normed, exw[...])
     margin = glog[:, 0:1] - glog[:, 1:2]
-    own_margin = jnp.where(chosen[:, 0:1] < n // GROUPS, margin, -margin)
+    own_margin = jnp.where(chosen[0] < n // GROUPS, margin, -margin)
     share = jax.nn.sigmoid(own_margin)
     eid = iota((tok, n), 1)
     picked = [
-        jnp.sum(jnp.where(chosen[:, i : i + 1] == eid, elog, 0.0), axis=1, keepdims=True)
+        jnp.sum(jnp.where(chosen[i] == eid, elog, 0.0), axis=1, keepdims=True)
         for i in range(2)
     ]
     route = [share * jax.nn.sigmoid(picked[i] - picked[1 - i]) for i in range(2)]
     slot_c = iota((tok, 2 * n), 1)
     exp_c = lax.div(slot_c, 2)
-    is_k = [chosen[:, i : i + 1] == exp_c for i in range(2)]
+    is_k = [chosen[i] == exp_c for i in range(2)]
     named_c = (is_k[0] | is_k[1]).astype(BF)
     before = (iota((tok, tok), 1) < iota((tok, tok), 0)).astype(BF)
     rank_c = dot(before, named_c)
@@ -512,7 +521,7 @@
         cols = slice(i * half, (i + 1) * half)
         bk = back[:, cols]
         mix = route[0] * dot(take[0], bk) + route[1] * dot(take[1], bk)
-        out[:, cols] = (mixed[:, cols].astype(F32) + mix).astype(BF)
+        out[:, cols] = mixed[:, cols].astype(F32) + mix
 
     for cond, copies in plan:
 
@@ -552,6 +561,9 @@
     dma = pltpu.SemaphoreType.DMA
     vm = pltpu.VMEM
     scratch = [
+        vm((tok, width), BF), vm((rows, att), BF), vm((rows, att), BF), vm((rows, att), BF),
+        vm((heads, rows), BF), vm((1, rows), jnp.int32), vm((1, width), F32),
+        vm((2, rows), jnp.int32),
         vm((n, rows, att), BF), vm((n, rows, att), BF), vm((n, 16, rows), BF), vm((16, rows), BF),
         vm((KB, KB), BF), vm((rows, att), BF), vm((rows, 1), F32), vm((rows, att), F32),
         vm((heads, rows, 1), F32),
@@ -565,8 +577,8 @@
         vm((2, 2 * nz, per, units), BF), vm((2 * nz, per, half), F32),
         vm((2, far, 2 * per, half), BF), vm((2, far, 2 * per, half), BF),
         vm((2, n, 2, half), BF), vm((2, n, 2, half), BF), vm((per, width), BF),
-        vm(group_router.shape, BF), vm(expert_router.shape, BF),
-        dma((6,)),
+        vm((GROUPS, width), BF), vm((n, width), BF),
+        dma((14,)),
         dma((sends,)), dma((n,)), dma((sends,)), dma((n,)), dma((sends,)), dma((n,)),
         dma((2,)), dma((2,)), dma, dma,
         dma((2, far, SUM_PIECES)), dma((2, far, SUM_PIECES)), dma, dma,
@@ -577,10 +589,10 @@
         dma((2, far, BACK_PIECES)), dma((2, far, BACK_PIECES)),
         dma((2, n)), dma((2, n)),
     ]
-    return pl.pallas_call(
+    summed = pl.pallas_call(
         functools.partial(layer_kernel, (ny, nx, nz)),
-        out_shape=jax.ShapeDtypeStruct(residual_in.shape, BF),
-        in_specs=[VM] * 6 + [ANY, VM, ANY, ANY, VM, ANY, ANY, ANY],
+        out_shape=jax.ShapeDtypeStruct(residual_in.shape, F32),
+        in_specs=[ANY] * 14,
         out_specs=VM,
         scratch_shapes=scratch,
         compiler_params=pltpu.CompilerParams(
@@ -588,9 +600,10 @@
         ),
         name="layer",
     )(
-        residual_in, queries, keys, values, break_offset, doc_ids[None, :], out_weight,
-        norm_gain[None, :], group_router, expert_router, expert_ids, gate, up, down,
+        residual_in, queries, keys, values, break_offset.T, doc_ids[None, :], out_weight,
+        norm_gain[None, :], group_router.T, expert_router.T, expert_ids.T, gate, up, down,
     )
+    return summed.astype(BF)
 
 
 def solution(mesh):

time: 128 us -> 117 us (0.914)
  local copies, waits for them, and re-layouts: 8.86 us -> 0 us
  Pallas kernels: 118 us -> 115 us
  other arithmetic: 0 us -> 1.62 us
    unnamed x5 -> x0, local copies, waits for them, and re-layouts: 8.86 us -> none
    pallas_call x1, Pallas kernels: 118 us -> 115 us  [per_device(): pl.pallas_call(functools.partial(layer_kernel, (ny, nx, nz)), out_shape=j...]
    convert_element_type x0 -> x1, other arithmetic: none -> 1.62 us  [per_device(): return summed.astype(BF)]
where the time goes in v3:
time: 117 us; the launch traced here: 116 us
  Pallas kernels  115 us (98%)
  other arithmetic  1.62 us (1%)
    pallas_call x1, Pallas kernels, per_device(): pl.pallas_call(functools.partial(layer_kernel, (ny, nx, nz)), out_shape=j...  115 us

profile of v3, /device:TPU:1, one launch (start us, length us, event | category | flops | bytes accessed | tf_op | source)
XLA Modules:
  0.0 116.5 jit_solution(10602180566186630477)
XLA Ops:
  0.0 114.8 %layer.1 = f32[16,4096]{1,0:T(8,128)} custom-call(bf16[16,4096]{1,0:T(8,128)(2,1)} %res_.1, bf16[256,128]{1,0:T(8,128)(2,1)} %q_.1, bf16[256,128]{1,0:T(8,128)(2,1)} %k_.1, bf16[256,128]{1,0:T(8,128)(2,1)} %v_.1, bf16[2,256]{1,0:T(2,128)(2,1)} %bitcast.16, s32[1,256]{1,0:T(1,128)} %bitcast.17, bf16[128,4096]{1,0:T(8,128)(2,1)} %w.1, f32[1,4096]{1,0:T(1,128)} %bitcast.13, ...), custom_call_target="tpu_custom_call" | custom-call | tf_op jit(solution)/shard_map/layer/pallas_call | solution.py:592
  114.8 1.6 %convert_element_type.3 = bf16[16,4096]{1,0:T(8,128)(2,1)} convert(f32[16,4096]{1,0:T(8,128)} %layer.1) | non-fusion elementwise | flops 65536 | bytes 393216 | tf_op jit(solution)/shard_map/convert_element_type | solution.py:606

commit v4 on v3

--- a/solution.py
+++ b/solution.py
@@ -17,6 +17,7 @@
 SUM_PIECES = 2
 ROW_PIECES = 4
 BACK_PIECES = 4
+NEAR = (0, 1, 3, 2)
 MESH = pl.DeviceIdType.MESH
 AXES = ("y", "x", "z", "c")
 SP = ("y", "x")
@@ -46,7 +47,7 @@
     )
 
 
-def attend_block(diag, q, kb, vb, ab, qd, acc, st, later):
+def attend_block(diag, q, kb, vb, ab, qd, part_out, part_go, later):
     heads = range(q.shape[1] // HEAD_DIM)
     rows = q.shape[0]
     cols = [slice(h * HEAD_DIM, (h + 1) * HEAD_DIM) for h in heads]
@@ -64,13 +65,8 @@
         log_w.append((s - go, dot(hi, later[...]) + dot(lo, later[...])))
     for h in heads:
         o = dot(jnp.exp(log_w[h][0] - log_w[h][1]).astype(BF), vb[:, cols[h]])
-        if diag:
-            acc[:, cols[h]] = o
-            st[h] = total[h]
-        else:
-            before = st[h]
-            acc[:, cols[h]] = acc[:, cols[h]] + jnp.exp(-before) * o
-            st[h] = before + total[h]
+        part_out[:, cols[h]] = o
+        part_go[h] = total[h]
 
 
 def layer_kernel(
@@ -78,7 +74,7 @@
     res_, q_, k_, v_, off_, doc_, w, gain_, grp, exr, ids_, gate, up, down,
     out,
     res, q, k, v, off, doc, gain, ids,
-    kall, vall, aall, auxo, later, qs, qd, acc, st,
+    kall, vall, aall, auxo, later, qs, qd, acc, st, run, tot_out,
     wown, wsib, att, pair, part, sbb, rbb, xbuf, ybuf, mixed,
     sent, inb, rows, gw, uw, dw, dsib, hid, partc, sbc, rbc, fin, ret, back, grw, exw,
     lsem, ks, kr, vs, vr, as_, ar, ws, wr, ds, dr, bs, br, es, er,
@@ -103,9 +99,11 @@
         sends.append(q_)
 
     others = []
-    for d in range(1, n):
-        t = lax.rem(me + d, n)
-        others.append((lax.div(t, nx), lax.rem(t, nx), t))
+    for dy in NEAR:
+        for dx in range(nx):
+            if dy or dx:
+                ty, tx = lax.rem(y + dy, ny), lax.rem(x + dx, nx)
+                others.append((ty, tx, ty * nx + tx))
     peers = [(ty, tx, z, c) for ty, tx, t in others]
     peers += [(ty, tx, z, 1 - c) for ty, tx, t in others]
     peers += [right, left, sib]
@@ -195,7 +193,7 @@
     start(remote(w.at[:, other_half], wsib, ws.at[0], wr.at[0], sib))
     start(remote(down.at[:, other_half], dsib, ws.at[1], wr.at[1], sib))
 
-    attend_block(True, qs, k, v, auxo, qd, acc, st, later)
+    attend_block(True, qs, k, v, auxo, qd, acc.at[me], st.at[me], later)
 
     firsts = []
     for i in range(max(nx, ny) - 1):
@@ -215,8 +213,7 @@
                 nv += 1
     del firsts
 
-    def step(t, carry):
-        b = me - t
+    def step(b):
         by = lax.div(b, nx)
         bx = lax.rem(b, nx)
 
@@ -231,12 +228,33 @@
                 a.wait_recv()
 
         attend_block(
-            False, qs, kall.at[b], vall.at[b], aall.at[b], qd, acc, st, later
+            False, qs, kall.at[b], vall.at[b], aall.at[b], qd, acc.at[b], st.at[b], later
         )
+
+    def walk(i, carry):
+        b = (y - lax.rem(i, ny)) * nx + lax.rem(x + nx - lax.div(i, ny), nx)
+
+        @pl.when((b >= 0) & used(b, me))
+        def _():
+            step(b)
+
         return carry
 
-    lax.fori_loop(1, jnp.minimum(me, BAND) + 1, step, 0)
-    att[...] = acc[...].astype(BF)
+    lax.fori_loop(1, n, walk, 0)
+    run[...] = st[me]
+    tot_out[...] = acc[me]
+
+    def gather(t, carry):
+        b = me - t
+        for h in range(heads):
+            hs = slice(h * HEAD_DIM, (h + 1) * HEAD_DIM)
+            before = run[h]
+            tot_out[:, hs] = tot_out[:, hs] + jnp.exp(-before) * acc[b, :, hs]
+            run[h] = before + st[b, h]
+        return carry
+
+    lax.fori_loop(1, jnp.minimum(me, BAND) + 1, gather, 0)
+    att[...] = tot_out[...].astype(BF)
     swap = remote(att, pair, ds, dr, sib)
     start(swap)
 
@@ -371,17 +389,16 @@
         jnp.where(is_k[i] & (rank_c == odd_c), 1.0, 0.0).astype(BF) for i in range(2)
     ]
 
-    for ty, tx, t in others:
-        remote(sent.at[t], inb.at[t], is_.at[0], ir.at[t], sib).wait_recv()
     mine = z * 2 + c
-    for e in range(n):
-        rows[mine, 2 * e : 2 * e + 2, :] = inb[e]
 
     per = rows.shape[1]
     hb = per // ROW_PIECES
 
+    def spot(p):
+        return pl.multiple_of(lax.rem(y + NEAR[p], ny) * hb, hb)
+
     def piece(b, p):
-        return rows.at[b, pl.ds(p * hb, hb), :]
+        return rows.at[b, pl.ds(spot(p), hb), :]
 
     def from_chip(d, h):
         return lax.rem(z + nz - h, nz) if d == 0 else lax.rem(z + h, nz)
@@ -407,15 +424,22 @@
         return list(range(hp)) if d == 0 else list(range(hp, ROW_PIECES))
 
     def order(d):
-        hp = ROW_PIECES // 2
-        a = list(range(hp))
-        b = list(range(hp, ROW_PIECES))
-        return a + b if d == 0 else b + a
-
-    for i in range(ROW_PIECES):
-        for d in (0, 1):
-            start(hop(d, 1, order(d)[i]))
+        return (0, 1, 2, 3) if d == 0 else (0, 2, 3, 1)
+
+    def out_pieces(k):
+        return [(0, k)] + {0: [(1, 0)], 1: [], 2: [(1, 2)], 3: [(1, 3), (1, 1)]}[k]
+
     for p in range(ROW_PIECES):
+        ty = lax.rem(y + NEAR[p], ny)
+        for dx in range(nx):
+            if NEAR[p] or dx:
+                t = ty * nx + lax.rem(x + dx, nx)
+                remote(sent.at[t], inb.at[t], is_.at[0], ir.at[t], sib).wait_recv()
+        rows[mine, pl.ds(spot(p), hb), :] = jnp.concatenate(
+            [inb[ty * nx + q_] for q_ in range(nx)], axis=0
+        )
+        for d, k_ in out_pieces(p):
+            start(hop(d, 1, k_))
         start(cross(0, 0, p, c))
 
     def blocks_of(h):
@@ -565,8 +589,8 @@
         vm((heads, rows), BF), vm((1, rows), jnp.int32), vm((1, width), F32),
         vm((2, rows), jnp.int32),
         vm((n, rows, att), BF), vm((n, rows, att), BF), vm((n, 16, rows), BF), vm((16, rows), BF),
-        vm((KB, KB), BF), vm((rows, att), BF), vm((rows, 1), F32), vm((rows, att), F32),
-        vm((heads, rows, 1), F32),
+        vm((KB, KB), BF), vm((rows, att), BF), vm((rows, 1), F32), vm((n, rows, att), F32),
+        vm((n, heads, rows, 1), F32), vm((heads, rows, 1), F32), vm((rows, att), F32),
         vm((att, half), BF), vm((att, half), BF), vm((rows, att), BF), vm((rows, att), BF),
         vm((rows, half), F32),
         vm((2, far, rows // nz, half), BF), vm((2, far, rows // nz, half), BF),

time: 117 us -> 116 us (level)
  no operation moved by 1% of the time
where the time goes in v4:
time: 116 us; the launch traced here: 115 us
  Pallas kernels  114 us (98%)
  other arithmetic  1.62 us (1%)
    pallas_call x1, Pallas kernels, per_device(): pl.pallas_call(functools.partial(layer_kernel, (ny, nx, nz)), out_shape=j...  114 us

profile of v4, /device:TPU:1, one launch (start us, length us, event | category | flops | bytes accessed | tf_op | source)
XLA Modules:
  0.0 115.5 jit_solution(4098188724421606583)
XLA Ops:
  0.0 113.8 %layer.1 = f32[16,4096]{1,0:T(8,128)} custom-call(bf16[16,4096]{1,0:T(8,128)(2,1)} %res_.1, bf16[256,128]{1,0:T(8,128)(2,1)} %q_.1, bf16[256,128]{1,0:T(8,128)(2,1)} %k_.1, bf16[256,128]{1,0:T(8,128)(2,1)} %v_.1, bf16[2,256]{1,0:T(2,128)(2,1)} %bitcast.16, s32[1,256]{1,0:T(1,128)} %bitcast.17, bf16[128,4096]{1,0:T(8,128)(2,1)} %w.1, f32[1,4096]{1,0:T(1,128)} %bitcast.13, ...), custom_call_target="tpu_custom_call" | custom-call | tf_op jit(solution)/shard_map/layer/pallas_call | solution.py:616
  113.8 1.6 %convert_element_type.3 = bf16[16,4096]{1,0:T(8,128)(2,1)} convert(f32[16,4096]{1,0:T(8,128)} %layer.1) | non-fusion elementwise | flops 65536 | bytes 393216 | tf_op jit(solution)/shard_map/convert_element_type | solution.py:630

commit v5 on v4

--- a/solution.py
+++ b/solution.py
@@ -14,7 +14,7 @@
 KB = 256
 BAND = DOC_MOST // KB
 NEG = -1e30
-SUM_PIECES = 2
+SUM_PIECES = 4
 ROW_PIECES = 4
 BACK_PIECES = 4
 NEAR = (0, 1, 3, 2)
@@ -258,7 +258,7 @@
     swap = remote(att, pair, ds, dr, sib)
     start(swap)
 
-    def ring_sum(own, sbuf, rbuf, s_sem, r_sem, np_, hr, last):
+    def ring_sum(own, sbuf, rbuf, s_sem, r_sem, np_, hr, last, begun=None):
         def move(d, s, p):
             ref = (d, s, pl.ds(p * hr, hr))
             return remote(
@@ -269,11 +269,11 @@
         def half_of(d):
             return range(np_ // 2) if d == 0 else range(np_ // 2, np_)
 
-        for s in range(far):
-            for i in range(np_ // 2 if s == 0 else np_):
+        for s in range(far) if begun is not False else (1,):
+            for i in range(np_ // 2 if s == 0 or (s == 1 and begun is not None) else np_):
                 for d in range(2):
                     order = list(half_of(d)) + ([] if s == 0 else list(half_of(1 - d)))
-                    p = order[i]
+                    p = order[i] if begun is not False else half_of(1 - d)[i]
                     dist = far - s
                     zz = lax.rem(z + dist, nz) if d == 0 else lax.rem(z + nz - dist, nz)
                     val = own(zz, p)
@@ -282,6 +282,8 @@
                         val = val + rbuf[d, s - 1, p * hr : (p + 1) * hr, :].astype(F32)
                     sbuf[d, s, p * hr : (p + 1) * hr, :] = val.astype(BF)
                     start(move(d, s, p))
+        if begun is False:
+            return
         for i in range(np_):
             p = i
             for d in range(2):
@@ -500,9 +502,6 @@
                     remote(down.at[:, other_half], dsib, ws.at[1], wr.at[1], sib).wait_recv()
             if i == 1:
                 finish(h - 1)
-    run(far)
-    finish(far)
-
     chunk_c = 2 * per
     hc = chunk_c // BACK_PIECES
 
@@ -531,7 +530,11 @@
                     fin.at[core, t], ret.at[c, me], fs.at[core, t], fr.at[c, me], sib
                 ).start()
 
-    ring_sum(own_c, sbc, rbc, ss, rs, BACK_PIECES, hc, last_c)
+    back_ring = (own_c, sbc, rbc, ss, rs, BACK_PIECES, hc, last_c)
+    ring_sum(*back_ring, begun=False)
+    run(far)
+    finish(far)
+    ring_sum(*back_ring, begun=True)
     ret[c, me] = fin[c, me]
     for i in (0, 1):
         for t in range(n):

time: 116 us -> 112 us (0.966)
  Pallas kernels: 114 us -> 111 us
    pallas_call x1, Pallas kernels: 114 us -> 111 us  [per_device(): pl.pallas_call(functools.partial(layer_kernel, (ny, nx, nz)), out_shape=j...]
where the time goes in v5:
time: 112 us
  Pallas kernels  111 us (99%)
  other arithmetic  1.62 us (1%)
    pallas_call x1, Pallas kernels, per_device(): pl.pallas_call(functools.partial(layer_kernel, (ny, nx, nz)), out_shape=j...  111 us

profile of v5, /device:TPU:1, one launch (start us, length us, event | category | flops | bytes accessed | tf_op | source)
XLA Modules:
  0.0 112.1 jit_solution(6048799704180161718)
XLA Ops:
  0.0 110.5 %layer.1 = f32[16,4096]{1,0:T(8,128)} custom-call(bf16[16,4096]{1,0:T(8,128)(2,1)} %res_.1, bf16[256,128]{1,0:T(8,128)(2,1)} %q_.1, bf16[256,128]{1,0:T(8,128)(2,1)} %k_.1, bf16[256,128]{1,0:T(8,128)(2,1)} %v_.1, bf16[2,256]{1,0:T(2,128)(2,1)} %bitcast.16, s32[1,256]{1,0:T(1,128)} %bitcast.17, bf16[128,4096]{1,0:T(8,128)(2,1)} %w.1, f32[1,4096]{1,0:T(1,128)} %bitcast.13, ...), custom_call_target="tpu_custom_call" | custom-call | tf_op jit(solution)/shard_map/layer/pallas_call | solution.py:619
  110.5 1.6 %convert_element_type.3 = bf16[16,4096]{1,0:T(8,128)(2,1)} convert(f32[16,4096]{1,0:T(8,128)} %layer.1) | non-fusion elementwise | flops 65536 | bytes 393216 | tf_op jit(solution)/shard_map/convert_element_type | solution.py:633

commit v6 on v5

--- a/solution.py
+++ b/solution.py
@@ -272,8 +272,11 @@
         for s in range(far) if begun is not False else (1,):
             for i in range(np_ // 2 if s == 0 or (s == 1 and begun is not None) else np_):
                 for d in range(2):
-                    order = list(half_of(d)) + ([] if s == 0 else list(half_of(1 - d)))
-                    p = order[i] if begun is not False else half_of(1 - d)[i]
+                    chained, fresh = list(half_of(d)), list(half_of(1 - d))
+                    if s == 0 or (s == 1 and begun):
+                        p = chained[i]
+                    else:
+                        p = (fresh + chained)[i]
                     dist = far - s
                     zz = lax.rem(z + dist, nz) if d == 0 else lax.rem(z + nz - dist, nz)
                     val = own(zz, p)

time: 112 us -> 110 us (0.982)
  Pallas kernels: 111 us -> 109 us
    pallas_call x1, Pallas kernels: 111 us -> 109 us  [per_device(): pl.pallas_call(functools.partial(layer_kernel, (ny, nx, nz)), out_shape=j...]
where the time goes in v6:
time: 110 us
  Pallas kernels  109 us (99%)
  other arithmetic  1.62 us (1%)
    pallas_call x1, Pallas kernels, per_device(): pl.pallas_call(functools.partial(layer_kernel, (ny, nx, nz)), out_shape=j...  109 us

profile of v6, /device:TPU:1, one launch (start us, length us, event | category | flops | bytes accessed | tf_op | source)
XLA Modules:
  0.0 110.2 jit_solution(17553229290695353761)
XLA Ops:
  0.0 108.6 %layer.1 = f32[16,4096]{1,0:T(8,128)} custom-call(bf16[16,4096]{1,0:T(8,128)(2,1)} %res_.1, bf16[256,128]{1,0:T(8,128)(2,1)} %q_.1, bf16[256,128]{1,0:T(8,128)(2,1)} %k_.1, bf16[256,128]{1,0:T(8,128)(2,1)} %v_.1, bf16[2,256]{1,0:T(2,128)(2,1)} %bitcast.16, s32[1,256]{1,0:T(1,128)} %bitcast.17, bf16[128,4096]{1,0:T(8,128)(2,1)} %w.1, f32[1,4096]{1,0:T(1,128)} %bitcast.13, ...), custom_call_target="tpu_custom_call" | custom-call | tf_op jit(solution)/shard_map/layer/pallas_call | solution.py:622
  108.6 1.6 %convert_element_type.3 = bf16[16,4096]{1,0:T(8,128)(2,1)} convert(f32[16,4096]{1,0:T(8,128)} %layer.1) | non-fusion elementwise | flops 65536 | bytes 393216 | tf_op jit(solution)/shard_map/convert_element_type | solution.py:636
